TPU v7x, 32 devices: a whole 2x2x4 slice. The times are simulated.
32 devices in a mesh: sp: 8 (over z, x), tp: 4 (over y, core).
Axes of the slice: x: 2, y: 2, z: 4, core: 2. Of those that a mesh axis runs over, the one named last changes fastest.
Arguments:
- queries: bfloat16 [3072, 768], P('sp', 'tp'), may hold values from -8 to 8
- keys: bfloat16 [3072, 256], P('sp', 'tp'), may hold values from -8 to 8
- values: bfloat16 [3072, 256], P('sp', 'tp'), may hold values from -6 to 6
- sinks: float32 [12], P('tp'), may hold values from 1 to 6
- residual: bfloat16 [3072, 2048], P('sp'), may hold values from -6 to 6
- out_weight: bfloat16 [768, 2048], replicated, may hold values from -3 to 3
- norm_gain: float32 [2048], replicated, may hold values from 0.1 to 1.9
- shared_gate: bfloat16 [2048, 512], P(None, 'tp'), may hold values from -0.125 to 0.125
- shared_up: bfloat16 [2048, 512], P(None, 'tp'), may hold values from -0.125 to 0.125
- shared_down: bfloat16 [512, 2048], P('tp'), may hold values from -0.25 to 0.25
- expert_ids: int32 [3072, 2], P('sp'), may hold values from 0 to 15, all different within a row; in each aligned block of 96 rows (0 to 95, 96 to 191, ...) at most 24 rows name the same one
- route_weights: float32 [3072, 2], P(('sp', 'tp')), may hold values from 0.2 to 2
- expert_gate: bfloat16 [16, 2048, 1024], P('sp', None, 'tp'), may hold values from -0.125 to 0.125
- expert_up: bfloat16 [16, 2048, 1024], P('sp', None, 'tp'), may hold values from -0.125 to 0.125
- expert_down: bfloat16 [16, 1024, 2048], P('sp', 'tp'), may hold values from -0.1875 to 0.1875
Outputs:
- layer_out: bfloat16 [3072, 2048], P(('sp', 'tp'))
Inputs may be any that keep to these rules, and one draw needn't show every extreme that they name: `expert_ids`: each row names 2 different experts. In each aligned block of 96 rows no expert is named more than 24 times, a bound that some blocks reach.
All inputs are finite; a program needn't handle non-finite values.
Results may differ from a plain program's by a relative error of at most 0.018.
Values may be sent and summed in bfloat16 or wider, within the bound.
A program may use at most 128 MiB of HBM per device.

v0:
```python
import jax
import jax.numpy as jnp
import numpy as np
from jax import lax
from jax.experimental import pallas as pl
from jax.experimental.pallas import tpu as pltpu
from jax.sharding import PartitionSpec as P
import functools

MESH = pl.DeviceIdType.MESH
VMEM = pl.BlockSpec(memory_space=pltpu.VMEM)
VMEM_LIMIT = 60 * 1024 * 1024

HEAD_DIM = 64
WINDOW = 128
GRID_W = 64
TOPK = 2


ROPE_BASE = 10000.0
NEG_LARGE = -1e30
NORM_EPSILON = 1e-06


def extended(x, sides, width):
    for axis, dim in sides:
        size, length = (lax.axis_size(axis), x.shape[dim])
        up = [(i, (i + 1) % size) for i in range(size - 1)]
        down = [(j, i) for i, j in up]
        last = lax.slice_in_dim(x, length - width, length, axis=dim)
        initial = lax.slice_in_dim(x, 0, width, axis=dim)
        before = lax.ppermute(last, axis, up)
        after = lax.ppermute(initial, axis, down)
        x = jnp.concatenate([before, x, after], axis=dim)
    return x


def rotary_turn(values, places):
    heads = values.shape[1] // HEAD_DIM
    halfway = HEAD_DIM // 2
    quarter = halfway // 2
    column = np.arange(HEAD_DIM)
    swap = np.zeros((HEAD_DIM, HEAD_DIM), np.float32)
    for d in range(HEAD_DIM):
        if d % halfway < quarter:
            swap[d + quarter, d] = -1.0
        else:
            swap[d - quarter, d] = 1.0
    swap = jnp.asarray(np.kron(np.eye(heads, dtype=np.float32), swap), jnp.bfloat16)
    spectrum = ROPE_BASE ** (-jnp.arange(0, halfway, 2, dtype=jnp.float32) / halfway)
    spectrum = jnp.tile(spectrum, values.shape[1] // quarter)
    first_half = jnp.asarray(np.tile(column < halfway, heads))
    offsets = jnp.where(
        first_half[None, :], (places // GRID_W)[:, None], (places % GRID_W)[:, None]
    )
    angles = offsets.astype(jnp.float32) * spectrum[None, :]
    swapped = jnp.dot(values, swap, preferred_element_type=jnp.float32)
    return (values.astype(jnp.float32) * jnp.cos(angles) + swapped * jnp.sin(angles)).astype(
        jnp.bfloat16
    )


def attend_kernel(key_heads, total_rows, first_ref, sink_ref, q_ref, kv_ref, out_ref):
    first = first_ref[0]
    heads = q_ref.shape[1] // HEAD_DIM
    group = heads // key_heads
    shape = (WINDOW, 3 * WINDOW)
    row = lax.broadcasted_iota(jnp.int32, shape, 0)
    column = lax.broadcasted_iota(jnp.int32, shape, 1) - WINDOW
    near = jnp.abs(row - column) <= WINDOW
    for block in range(q_ref.shape[0] // WINDOW):
        start = block * WINDOW
        key_at = column + (first + start)
        allowed = near & (key_at >= 0) & (key_at < total_rows)
        for kh in range(key_heads):
            span = slice(start, start + 3 * WINDOW)
            key = kv_ref[span, kh * HEAD_DIM : (kh + 1) * HEAD_DIM]
            value = kv_ref[span, (key_heads + kh) * HEAD_DIM : (key_heads + kh + 1) * HEAD_DIM]
            for h in range(kh * group, (kh + 1) * group):
                query = q_ref[start : start + WINDOW, h * HEAD_DIM : (h + 1) * HEAD_DIM]
                scores = lax.dot_general(
                    query, key, (((1,), (1,)), ((), ())), preferred_element_type=jnp.float32
                ) * HEAD_DIM ** (-0.5)
                scores = jnp.where(allowed, scores, NEG_LARGE)
                sink = sink_ref[h]
                highest = jnp.maximum(jnp.max(scores, axis=1, keepdims=True), sink)
                lifted = jnp.exp(scores - highest)
                below = jnp.sum(lifted, axis=1, keepdims=True) + jnp.exp(sink - highest)
                chances = (lifted / below).astype(jnp.bfloat16)
                result = jnp.dot(chances, value, preferred_element_type=jnp.float32)
                out_ref[start : start + WINDOW, h * HEAD_DIM : (h + 1) * HEAD_DIM] = result.astype(
                    jnp.bfloat16
                )


def attend(first, sinks, turned, widened, key_heads, total_rows):
    smem = pl.BlockSpec(memory_space=pltpu.SMEM)
    return pl.pallas_call(
        functools.partial(attend_kernel, key_heads, total_rows),
        out_shape=jax.ShapeDtypeStruct(turned.shape, jnp.bfloat16),
        in_specs=[smem, smem, VMEM, VMEM],
        out_specs=VMEM,
        name="attend",
    )(first.reshape(1), sinks, turned, widened)


def routes_kernel(capacity, ids_ref, ids_row_ref, weights_ref, sender_ref, weigh_ref):
    own, slot_count = sender_ref.shape
    earlier = lax.broadcasted_iota(jnp.int32, (own, own), 1) < lax.broadcasted_iota(
        jnp.int32, (own, own), 0
    )
    slot_of = lax.broadcasted_iota(jnp.int32, (own, slot_count), 1)
    taken = jnp.zeros((own, slot_count), jnp.float32)
    weigh = jnp.zeros((own, slot_count), jnp.float32)
    for k in range(TOPK):
        mine = ids_ref[:, k : k + 1]
        rank = jnp.zeros((own, 1), jnp.int32)
        for other in range(TOPK):
            same = (ids_row_ref[other : other + 1, :] == mine) & earlier
            rank = rank + jnp.sum(same.astype(jnp.int32), axis=1, keepdims=True)
        chosen = slot_of == mine * capacity + rank
        taken = jnp.where(chosen, 1.0, taken)
        weigh = jnp.where(chosen, weights_ref[:, k : k + 1], weigh)
    sender_ref[...] = taken.astype(jnp.bfloat16)
    coarse = weigh.astype(jnp.bfloat16)
    weigh_ref[:own, :] = coarse
    weigh_ref[own:, :] = (weigh - coarse.astype(jnp.float32)).astype(jnp.bfloat16)


def routes(own_ids, weights, capacity, slot_count):
    own = own_ids.shape[0]
    return pl.pallas_call(
        functools.partial(routes_kernel, capacity),
        out_shape=(
            jax.ShapeDtypeStruct((own, slot_count), jnp.bfloat16),
            jax.ShapeDtypeStruct((2 * own, slot_count), jnp.bfloat16),
        ),
        in_specs=[VMEM] * 3,
        out_specs=(VMEM, VMEM),
        name="routes",
    )(own_ids, own_ids.T, weights)


def gated_hidden(gathered_rows, gate_weight, up_weight):
    gate_values = jnp.dot(gathered_rows, gate_weight, preferred_element_type=jnp.float32)
    up_values = jnp.dot(gathered_rows, up_weight, preferred_element_type=jnp.float32)
    return (jax.nn.silu(gate_values) * up_values).astype(jnp.bfloat16)


def places_of(token_split, width_split):
    sp_at = lax.axis_index("sp")
    tp_at = lax.axis_index("tp")
    pair = tp_at + 1 - 2 * (tp_at % 2)
    cross = (tp_at + width_split // 2) % width_split
    return sp_at, tp_at, pair, cross


def greet(token_split, sp_at, tp_at, pair, cross):
    barrier = pltpu.get_barrier_semaphore()

    @pl.loop(1, token_split)
    def _(i):
        pl.semaphore_signal(
            barrier, inc=1, device_id=((sp_at + i) % token_split, tp_at), device_id_type=MESH
        )

    for partner in (pair, cross):
        pl.semaphore_signal(barrier, inc=1, device_id=(sp_at, partner), device_id_type=MESH)
    pl.semaphore_wait(barrier, token_split + 1)


def dispatch_kernel(
    token_split,
    width_split,
    rows_ref,
    normed_ref,
    gate_ref,
    up_ref,
    down_ref,
    out_ref,
    shared_ref,
    local_sem,
    send,
    recv,
):
    sp_at, tp_at, pair, cross = places_of(token_split, width_split)
    greet(token_split, sp_at, tp_at, pair, cross)

    def remote(stage, i, source, target, where):
        return pltpu.make_async_remote_copy(
            src_ref=source,
            dst_ref=target,
            send_sem=send.at[stage, i],
            recv_sem=recv.at[stage, i],
            device_id=where,
            device_id_type=MESH,
        )

    def along(i):
        there = (sp_at + i) % token_split
        return remote(0, i, rows_ref.at[there], out_ref.at[:, tp_at, sp_at], (there, tp_at))

    def passed(stage, i, block, partner):
        piece = out_ref.at[:, block, (sp_at + token_split - i) % token_split]
        return remote(stage, i, piece, piece, (sp_at, partner))

    @pl.loop(1, token_split)
    def _(i):
        along(i).start()

    own = pltpu.make_async_copy(rows_ref.at[sp_at], out_ref.at[:, tp_at, sp_at], local_sem)
    own.start()
    own.wait()
    passed(1, 0, tp_at, cross).start()
    passed(2, 0, tp_at, pair).start()

    @pl.loop(1, token_split)
    def _(i):
        along(i).wait_recv()
        passed(1, i, tp_at, cross).start()
        passed(2, i, tp_at, pair).start()

    own_rows = shared_ref.shape[1]
    for block in range(width_split):
        here = normed_ref[block * own_rows : (block + 1) * own_rows, :]
        hidden = gated_hidden(here, gate_ref[...], up_ref[...])
        shared_ref[block] = jnp.dot(
            hidden, down_ref[...], preferred_element_type=jnp.float32
        ).astype(shared_ref.dtype)

    @pl.loop(0, token_split)
    def _(i):
        passed(1, i, tp_at, cross).wait_recv()
        passed(3, i, cross, pair).start()

    @pl.loop(0, token_split)
    def _(i):
        passed(2, i, tp_at, pair).wait()
        passed(1, i, tp_at, cross).wait_send()
        passed(3, i, cross, pair).wait()

    @pl.loop(1, token_split)
    def _(i):
        along(i).wait_send()


def dispatch(rows, normed, gate, up, down, token_split, width_split):
    _, experts, cap, width = rows.shape
    return pl.pallas_call(
        functools.partial(dispatch_kernel, token_split, width_split),
        out_shape=(
            jax.ShapeDtypeStruct((experts, width_split, token_split, cap, width), rows.dtype),
            jax.ShapeDtypeStruct(
                (width_split, normed.shape[0] // width_split, width), rows.dtype
            ),
        ),
        in_specs=[VMEM] * 5,
        out_specs=(VMEM, VMEM),
        scratch_shapes=[
            pltpu.SemaphoreType.DMA,
            pltpu.SemaphoreType.DMA((4, token_split)),
            pltpu.SemaphoreType.DMA((4, token_split)),
        ],
        compiler_params=pltpu.CompilerParams(
            collective_id=1, has_side_effects=True, vmem_limit_bytes=VMEM_LIMIT
        ),
        name="dispatch",
    )(rows, normed, gate, up, down)


def collect_kernel(
    token_split,
    width_split,
    part_ref,
    shared_ref,
    back_ref,
    shared_out,
    from_pair,
    to_cross,
    from_cross,
    final,
    shared_pair,
    shared_cross,
    shared_got,
    send,
    recv,
    shared_send,
    shared_recv,
):
    sp_at, tp_at, pair, cross = places_of(token_split, width_split)
    pair_cross = (pair + width_split // 2) % width_split
    greet(token_split, sp_at, tp_at, pair, cross)

    def copy(source, target, sems, where):
        return pltpu.make_async_remote_copy(
            src_ref=source,
            dst_ref=target,
            send_sem=sems[0],
            recv_sem=sems[1],
            device_id=where,
            device_id_type=MESH,
        )

    def at(stage, i):
        return send.at[stage, i], recv.at[stage, i]

    def at_shared(stage):
        return shared_send.at[stage], shared_recv.at[stage]

    def place(i):
        return (sp_at + 1 + i) % token_split

    def pair_copy(side, i):
        block = pair_cross if side == 0 else pair
        there = place(i)
        return copy(
            part_ref.at[:, block, there], from_pair.at[side, there], at(side, i), (sp_at, pair)
        )

    def cross_copy(i):
        there = place(i)
        return copy(to_cross.at[there], from_cross.at[there], at(2, i), (sp_at, cross))

    def along_copy(i):
        there = place(i)
        return copy(final.at[there], back_ref.at[sp_at], at(3, i), (there, tp_at))

    def shared_copy(side):
        block = pair_cross if side == 0 else pair
        return copy(shared_ref.at[block], shared_pair.at[side], at_shared(side), (sp_at, pair))

    shared_over = copy(shared_cross, shared_got, at_shared(2), (sp_at, cross))

    @pl.loop(0, token_split)
    def _(i):
        pair_copy(0, i).start()

    shared_copy(0).start()

    @pl.loop(0, token_split)
    def _(i):
        pair_copy(1, i).start()

    shared_copy(1).start()

    def total(*terms):
        value = terms[0].astype(jnp.float32)
        for term in terms[1:]:
            value = value + term.astype(jnp.float32)
        return value

    @pl.loop(0, token_split)
    def _(i):
        there = place(i)
        pair_copy(0, i).wait_recv()
        to_cross[there] = total(part_ref[:, cross, there], from_pair[0, there]).astype(
            to_cross.dtype
        )
        cross_copy(i).start()

    shared_copy(0).wait_recv()
    shared_cross[...] = total(shared_ref[cross], shared_pair[0]).astype(shared_cross.dtype)
    shared_over.start()

    def summed(i):
        there = place(i)
        pair_copy(1, i).wait_recv()
        cross_copy(i).wait_recv()
        return total(part_ref[:, tp_at, there], from_pair[1, there], from_cross[there]).astype(
            back_ref.dtype
        )

    @pl.loop(0, token_split - 1)
    def _(i):
        final[place(i)] = summed(i)
        along_copy(i).start()

    back_ref[sp_at] = summed(token_split - 1)
    shared_copy(1).wait_recv()
    shared_over.wait_recv()
    shared_out[...] = total(shared_ref[tp_at], shared_pair[1], shared_got[...])

    @pl.loop(0, token_split)
    def _(i):
        pair_copy(0, i).wait_send()
        pair_copy(1, i).wait_send()
        cross_copy(i).wait_send()

    shared_copy(0).wait_send()
    shared_copy(1).wait_send()
    shared_over.wait_send()

    @pl.loop(0, token_split - 1)
    def _(i):
        along_copy(i).wait()


def collect(part, shared, token_split, width_split):
    experts, _, _, cap, width = part.shape
    own = shared.shape[1]
    block = (token_split, experts, cap, width)
    kind = part.dtype
    return pl.pallas_call(
        functools.partial(collect_kernel, token_split, width_split),
        out_shape=(
            jax.ShapeDtypeStruct(block, kind),
            jax.ShapeDtypeStruct((own, width), jnp.float32),
        ),
        in_specs=[VMEM] * 2,
        out_specs=(VMEM, VMEM),
        scratch_shapes=[
            pltpu.VMEM((2,) + block, kind),
            pltpu.VMEM(block, kind),
            pltpu.VMEM(block, kind),
            pltpu.VMEM(block, kind),
            pltpu.VMEM((2, own, width), kind),
            pltpu.VMEM((own, width), kind),
            pltpu.VMEM((own, width), kind),
            pltpu.SemaphoreType.DMA((4, token_split)),
            pltpu.SemaphoreType.DMA((4, token_split)),
            pltpu.SemaphoreType.DMA((3,)),
            pltpu.SemaphoreType.DMA((3,)),
        ],
        compiler_params=pltpu.CompilerParams(
            collective_id=2, has_side_effects=True, vmem_limit_bytes=VMEM_LIMIT
        ),
        name="collect",
    )(part, shared)


def per_device(
    queries,
    keys,
    values,
    sinks,
    residual,
    out_weight,
    norm_gain,
    shared_gate,
    shared_up,
    shared_down,
    expert_ids,
    route_weights,
    expert_gate,
    expert_up,
    expert_down,
):
    block_rows = queries.shape[0]
    width_split = lax.axis_size("tp")
    token_split = lax.axis_size("sp")
    width_index = lax.axis_index("tp")
    key_heads = keys.shape[1] // HEAD_DIM
    heads_local = queries.shape[1] // HEAD_DIM
    first_row = lax.axis_index("sp") * block_rows
    total_rows = token_split * block_rows
    places = first_row + jnp.arange(block_rows, dtype=jnp.int32)
    turned = rotary_turn(jnp.concatenate([queries, keys], axis=1), places)
    query_width = heads_local * HEAD_DIM
    joined = jnp.concatenate([turned[:, query_width:], values], axis=1)
    widened = extended(joined, (("sp", 0),), WINDOW)
    attended = attend(
        first_row, sinks, turned[:, :query_width], widened, key_heads, total_rows
    )
    model_width = out_weight.shape[1]
    projected = jnp.dot(
        lax.all_gather(attended, "tp", axis=1, tiled=True),
        out_weight,
        preferred_element_type=jnp.float32,
    )
    mixed_rows = (residual.astype(jnp.float32) + projected).astype(jnp.bfloat16)
    mixed_float = mixed_rows.astype(jnp.float32)
    scale_rows = lax.rsqrt(
        jnp.mean(mixed_float * mixed_float, axis=-1, keepdims=True) + NORM_EPSILON
    )
    normed = (mixed_float * scale_rows * norm_gain).astype(jnp.bfloat16)
    own_rows = block_rows // width_split
    experts_here = expert_gate.shape[0]
    experts_all = experts_here * token_split
    capacity = max(2, 2 * own_rows * TOPK // experts_all)
    own_start = width_index * own_rows
    own_ids = lax.dynamic_slice_in_dim(expert_ids, own_start, own_rows, 0)
    slot_count = experts_all * capacity
    sender, weigh = routes(own_ids, route_weights, capacity, slot_count)
    normed_own = lax.dynamic_slice_in_dim(normed, own_start, own_rows, 0)
    outgoing = lax.dot_general(
        sender, normed_own, (((0,), (0,)), ((), ())), preferred_element_type=jnp.float32
    ).astype(jnp.bfloat16)
    outgoing = outgoing.reshape(token_split, experts_here, capacity, model_width)
    arrived, shared_part = dispatch(
        outgoing, normed, shared_gate, shared_up, shared_down, token_split, width_split
    )
    slot_batch = arrived.reshape(experts_here, -1, model_width)
    gate_values = jnp.einsum(
        "erd,edh->erh", slot_batch, expert_gate, preferred_element_type=jnp.float32
    )
    up_values = jnp.einsum(
        "erd,edh->erh", slot_batch, expert_up, preferred_element_type=jnp.float32
    )
    hidden = (jax.nn.silu(gate_values) * up_values).astype(jnp.bfloat16)
    partial_value = jnp.einsum(
        "erh,ehd->erd", hidden, expert_down, preferred_element_type=jnp.float32
    ).astype(jnp.bfloat16)
    returned, shared_sum = collect(
        partial_value.reshape(arrived.shape), shared_part, token_split, width_split
    )
    flat_back = returned.reshape(slot_count, model_width)
    routed = jnp.dot(weigh, flat_back, preferred_element_type=jnp.float32)
    routed = routed[:own_rows] + routed[own_rows:]
    mixed_own = lax.dynamic_slice_in_dim(mixed_float, own_start, own_rows, 0)
    return (mixed_own + shared_sum + routed).astype(jnp.bfloat16)


def solution(mesh):
    placed = (
        P("sp", "tp"),
        P("sp", "tp"),
        P("sp", "tp"),
        P("tp"),
        P("sp", None),
        P(),
        P(),
        P(None, "tp"),
        P(None, "tp"),
        P("tp", None),
        P("sp", None),
        P(("sp", "tp"), None),
        P("sp", None, "tp"),
        P("sp", None, "tp"),
        P("sp", "tp", None),
    )
    return jax.shard_map(
        per_device, mesh=mesh, in_specs=placed, out_specs=P(("sp", "tp"), None), check_vma=False
    )
```

profile of v0, /device:TPU:0, one launch (start us, length us, event | category | flops | bytes accessed | tf_op | source)
XLA Modules:
  0.0 184.4 jit_solution(4368682379730596880)
XLA Ops:
  0.0 0.0 copy-start
  0.0 0.0 copy-start.8
  0.0 0.0 copy-start.9
  0.1 0.7 mul.57
  0.7 1.0 copy.29
  1.7 0.9 copy.26
  2.6 1.7 copy.25
  4.4 1.2 fusion.14
  5.6 2.7 %fusion.4 = bf16[384,256]{1,0:T(8,128)(2,1)S(1)} fusion(f32[256,384]{0,1:T(8,128)S(1)} %fusion.14, bf16[64,256]{1,0:T(8,128)(2,1)} %constant.70, bf16[384,64]{0,1:T(8,128)(2,1)} %param.18, bf16[384,64]{1,0:T(8,128)(2,1)S(1)} %copy.26, bf16[384,192]{1,0:T(8,128)(2,1)} %copy.25, f32[256]{0:T(256)} %mul.57, s32[384]{0:T(512)S(1)} %get-tuple-element.21, ...), kind=kOutput, calls=%fused_computation.11 | convolution fusion | flops 13762560 | bytes 872704 | tf_op jit(solution)/shard_map/dot_general | solution.py:57
  8.3 0.0 copy-start.4
  8.3 0.1 slice.27
  8.4 0.7 pad_maximum_fusion.2
  9.1 5.5 %collective-permute-start = (bf16[128,128]{1,0:T(8,128)(2,1)}, bf16[128,128]{1,0:T(8,128)(2,1)}, u32[]{:S(2)}, u32[]{:S(2)}) collective-permute-start(bf16[128,128]{1,0:T(8,128)(2,1)} %get-tuple-element.17), channel_id=1, source_target_pairs={{0,4},{4,8},{8,12},{12,16},{16,20},{20,24},{24,28},{1,5},{5,9},{9,... | collective-permute-start | bytes 98312 | tf_op jit(solution)/shard_map/ppermute | solution.py:32
  14.6 1.3 collective-permute-start.1
  15.9 0.0 copy-done.8
  15.9 0.6 fusion.31.ids_row_ref
  16.5 0.1 constant_dynamic-slice_fusion
  16.6 0.7 copy.31.ids_ref
  17.3 0.0 copy-done.9
  17.3 0.7 copy.32.weights_ref
  18.0 2.0 %routes.1 = (bf16[96,384]{1,0:T(8,128)(2,1)}, bf16[192,384]{1,0:T(8,128)(2,1)}) custom-call(s32[96,2]{1,0:T(8,128)} %copy.31.ids_ref, s32[2,96]{1,0:T(2,128)} %fusion.31.ids_row_ref, f32[96,2]{1,0:T(8,128)} %copy.32.weights_ref), custom_call_target="tpu_custom_call" | custom-call | tf_op jit(solution)/shard_map/routes/pallas_call | solution.py:132
  20.0 0.0 collective-permute-done
  20.0 0.7 collective-permute-done.1
  20.7 1.5 pad_maximum_fusion.kv_ref
  22.2 0.0 copy-done.4
  22.2 5.0 %attend.1 = bf16[384,192]{1,0:T(8,128)(2,1)} custom-call(s32[1]{0:T(128)} %bitcast.first_ref, f32[3]{0:T(128)} %sink_ref.1, bf16[384,192]{1,0:T(8,128)(2,1)} %bitcast.33, bf16[640,128]{1,0:T(8,128)(2,1)} %pad_maximum_fusion.kv_ref), custom_call_target="tpu_custom_call" | custom-call | tf_op jit(solution)/shard_map/attend/pallas_call | solution.py:98
  27.3 1.1 copy.30
  28.3 7.7 %all_gather.3 = bf16[384,768]{0,1:T(8,128)(2,1)S(1)} all-gather(bf16[384,192]{0,1:T(8,128)(2,1)S(1)} %copy.30), channel_id=1, replica_groups=mesh['sp'=8,'tp'=4] {'tp'}, dimensions={1}, use_global_device_ids=true | all-gather | bytes 737280 | tf_op jit(solution)/shard_map/all_gather | solution.py:466
  36.1 0.0 copy-done
  36.1 0.0 copy-start.7
  36.1 3.2 %multiply_reduce_fusion = (f32[384]{0:T(512)S(1)}, f32[384,2048]{1,0:T(8,128)S(1)}) fusion(bf16[384,768]{0,1:T(8,128)(2,1)S(1)} %all_gather.3, bf16[768,2048]{1,0:T(8,128)(2,1)S(1)} %copy-done, bf16[384,2048]{1,0:T(8,128)(2,1)} %param.21), kind=kOutput, calls=%fused_computation.2 | convolution fusion | flops 1212677760 | bytes 8455680 | tf_op jit(solution)/shard_map/dot_general | solution.py:465
  39.2 0.0 copy-start.1
  39.2 0.0 copy-done.7
  39.3 0.0 copy-start.6
  39.3 0.3 multiply_convert_fusion.normed_ref
  39.6 1.3 copy-done.1
  40.9 1.1 copy-done.2
  42.0 0.0 copy-done.6
  42.0 1.8 convolution_convert_fusion.1
  43.9 57.1 %dispatch.1 = (bf16[2,4,8,24,2048]{4,3,2,1,0:T(8,128)(2,1)}, bf16[4,96,2048]{2,1,0:T(8,128)(2,1)}) custom-call(bf16[8,2,24,2048]{3,2,1,0:T(8,128)(2,1)} %bitcast.30, bf16[384,2048]{1,0:T(8,128)(2,1)} %copy-done.2, bf16[2048,128]{1,0:T(8,128)(2,1)} %gate_ref.1, bf16[2048,128]{1,0:T(8,128)(2,1)} %up_ref.1, bf16[128,2048]{1,0:T(8,128)(2,1)} %down_ref.1), custom_call_target="tpu_custom_call" | custom-call | tf_op jit(solution)/shard_map/dispatch/pallas_call | solution.py:249
  101.0 6.4 %fusion.15 = f32[2,768,256]{2,1,0:T(8,128)} fusion(bf16[2,768,2048]{2,1,0:T(8,128)(2,1)} %bitcast.34, bf16[2,2048,256]{2,1,0:T(8,128)(2,1)} %param.29), kind=kOutput, calls=%fused_computation.36 | convolution fusion | flops 1610612736 | bytes 9961472 | tf_op jit(solution)/shard_map/erd,edh->erh/dot_general | solution.py:493
  107.3 10.7 %convolution_convert_fusion = bf16[2,768,2048]{2,1,0:T(8,128)(2,1)} fusion(bf16[2,256,2048]{2,1,0:T(8,128)(2,1)} %param.31, f32[2,768,256]{2,1,0:T(8,128)} %fusion.15, bf16[2,768,2048]{2,1,0:T(8,128)(2,1)} %bitcast.35, bf16[2,2048,256]{2,1,0:T(8,128)(2,1)} %param.30), kind=kOutput, calls=%fused_computation | convolution fusion | flops 3226730496 | bytes 18350080 | tf_op jit(solution)/shard_map/erh,ehd->erd/dot_general | solution.py:500
  118.0 62.1 %collect.1 = (bf16[8,2,24,2048]{3,2,1,0:T(8,128)(2,1)}, f32[96,2048]{1,0:T(8,128)}) custom-call(bf16[2,4,8,24,2048]{4,3,2,1,0:T(8,128)(2,1)} %bitcast.31, bf16[4,96,2048]{2,1,0:T(8,128)(2,1)} %get-tuple-element.13.shared_ref), custom_call_target="tpu_custom_call" | custom-call | tf_op jit(solution)/shard_map/collect/pallas_call | solution.py:403
  180.2 0.0 copy-start.3
  180.2 0.0 copy-done.5
  180.2 2.0 %fusion.16 = f32[192,2048]{1,0:T(8,128)S(1)} fusion(bf16[192,384]{1,0:T(8,128)(2,1)S(1)} %copy-done.5, bf16[384,2048]{1,0:T(8,128)(2,1)} %bitcast.32), kind=kOutput, calls=%fused_computation.37 | convolution fusion | flops 301989888 | bytes 3293184 | tf_op jit(solution)/shard_map/dot_general | solution.py:507
  182.3 0.0 copy-done.3
  182.3 2.1 %fusion.6 = bf16[96,2048]{1,0:T(8,128)(2,1)} fusion(f32[192,2048]{1,0:T(8,128)S(1)} %fusion.16, f32[96,2048]{1,0:T(8,128)S(1)} %copy-done.3, f32[384,2048]{1,0:T(8,128)} %copy-done.1, s32[]{:T(128)S(6)} %select_n.32), kind=kLoop, calls=%fused_computation.14 | loop fusion | flops 786432 | bytes 3538948 | tf_op jit(solution)/shard_map/convert_element_type | solution.py:510
  (6 shorter events, 0.0 us)
Async XLA Ops:
  0.0 36.1 %copy-start = (bf16[768,2048]{1,0:T(8,128)(2,1)S(1)}, bf16[768,2048]{1,0:T(8,128)(2,1)}, u32[]{:S(2)}) copy-start(bf16[768,2048]{1,0:T(8,128)(2,1)} %param.22) | copy-start | bytes 9437188
  0.0 15.9 %copy-start.8 = (s32[384,2]{0,1:T(2,128)S(1)}, s32[384,2]{0,1:T(2,128)}, u32[]{:S(2)}) copy-start(s32[384,2]{0,1:T(2,128)} %param.27) | copy-start | bytes 9220
  0.0 17.3 %copy-start.9 = (f32[96,2]{0,1:T(2,128)S(1)}, f32[96,2]{0,1:T(2,128)}, u32[]{:S(2)}) copy-start(f32[96,2]{0,1:T(2,128)} %param.28) | copy-start | bytes 2308
  8.3 14.0 %copy-start.4 = (bf16[384,256]{1,0:T(8,128)(2,1)}, bf16[384,256]{1,0:T(8,128)(2,1)S(1)}, u32[]{:S(2)}) copy-start(bf16[384,256]{1,0:T(8,128)(2,1)S(1)} %fusion.4) | copy-start | bytes 589828
  9.1 10.9 %collective-permute-start = (bf16[128,128]{1,0:T(8,128)(2,1)}, bf16[128,128]{1,0:T(8,128)(2,1)}, u32[]{:S(2)}, u32[]{:S(2)}) collective-permute-start(bf16[128,128]{1,0:T(8,128)(2,1)} %get-tuple-element.17), channel_id=1, source_target_pairs={{0,4},{4,8},{8,12},{12,16},{16,20},{20,24},{24,28},{1,5},{5,9},{9,... | collective-permute-start | bytes 98312 | tf_op jit(solution)/shard_map/ppermute | solution.py:32
  14.6 6.1 %collective-permute-start.1 = (bf16[128,128]{1,0:T(8,128)(2,1)}, bf16[128,128]{1,0:T(8,128)(2,1)}, u32[]{:S(2)}, u32[]{:S(2)}) collective-permute-start(bf16[128,128]{1,0:T(8,128)(2,1)} %get-tuple-element.18), channel_id=1, source_target_pairs={{4,0},{8,4},{12,8},{16,12},{20,16},{24,20},{28,24},{5,1},{9,5},{13... | collective-permute-start | bytes 98312 | tf_op jit(solution)/shard_map/ppermute | solution.py:33
  36.1 3.2 %copy-start.7 = (f32[2048]{0:T(1024)S(1)}, f32[2048]{0:T(1024)}, u32[]{:S(2)}) copy-start(f32[2048]{0:T(1024)} %param.23) | copy-start | bytes 24580
  39.2 1.7 copy-start.1
  39.3 2.8 %copy-start.6 = (bf16[96,384]{1,0:T(8,128)(2,1)S(1)}, bf16[96,384]{1,0:T(8,128)(2,1)}, u32[]{:S(2)}) copy-start(bf16[96,384]{1,0:T(8,128)(2,1)} %get-tuple-element.11) | copy-start | bytes 221188
  40.9 1.1 copy-start.2
  118.0 62.2 %copy-start.5 = (bf16[192,384]{1,0:T(8,128)(2,1)S(1)}, bf16[192,384]{1,0:T(8,128)(2,1)}, u32[]{:S(2)}) copy-start(bf16[192,384]{1,0:T(8,128)(2,1)} %get-tuple-element.15) | copy-start | bytes 442372
  180.2 2.1 %copy-start.3 = (f32[96,2048]{1,0:T(8,128)S(1)}, f32[96,2048]{1,0:T(8,128)}, u32[]{:S(2)}) copy-start(f32[96,2048]{1,0:T(8,128)} %get-tuple-element.14) | copy-start | bytes 2359300
where the time goes:
time: 185 us; the launch traced here: 184 us
  Pallas kernels  126 us (68%)
  matrix products  28 us (15%)
  local copies, waits for them, and re-layouts  10.1 us (5%)
  blocking collectives  7.73 us (4%)
  starting transfers between devices  6.77 us (4%)
  other arithmetic  4.71 us (3%)
    pallas_call x1, Pallas kernels, collect(): pl.pallas_call(functools.partial(collect_kernel, token_split, width_split...  62.1 us
    pallas_call x1, Pallas kernels, dispatch(): pl.pallas_call(functools.partial(dispatch_kernel, token_split, width_spli...  57.1 us
    dot_general x1, matrix products, per_device(): jnp.einsum('erh,ehd->erd', hidden, expert_down, preferred_element_type=jn...  10.7 us
    all_gather x1, blocking collectives, per_device(): lax.all_gather(attended, 'tp', axis=1, tiled=True)  7.73 us
    unnamed x24, local copies, waits for them, and re-layouts  6.84 us
    dot_general x1, matrix products, per_device(): jnp.einsum('erd,edh->erh', slot_batch, expert_gate, preferred_element_typ...  6.38 us
    ppermute x1, starting transfers between devices, extended(): before = lax.ppermute(last, axis, up)  5.49 us
    pallas_call x1, Pallas kernels, attend(): pl.pallas_call(functools.partial(attend_kernel, key_heads, total_rows), o...  5.02 us
  transfers between devices with their start and end apart: 2, of which 1 were waited for; matrix products, arithmetic and copies ran while one was open for 1% of the time, Pallas kernels for 1%

commit v1 on v0

v1 whole, which is shorter than its diff:
```python
import jax
import jax.numpy as jnp
import numpy as np
from jax import lax
from jax.experimental import pallas as pl
from jax.experimental.pallas import tpu as pltpu
from jax.sharding import PartitionSpec as P
import functools

MESH = pl.DeviceIdType.MESH
VMEM = pl.BlockSpec(memory_space=pltpu.VMEM)
VMEM_LIMIT = 60 * 1024 * 1024

HEAD_DIM = 64
WINDOW = 128
GRID_W = 64
TOPK = 2


ROPE_BASE = 10000.0
NEG_LARGE = -1e30
NORM_EPSILON = 1e-06


def extended(x, sides, width):
    for axis, dim in sides:
        size, length = (lax.axis_size(axis), x.shape[dim])
        up = [(i, (i + 1) % size) for i in range(size - 1)]
        down = [(j, i) for i, j in up]
        last = lax.slice_in_dim(x, length - width, length, axis=dim)
        initial = lax.slice_in_dim(x, 0, width, axis=dim)
        before = lax.ppermute(last, axis, up)
        after = lax.ppermute(initial, axis, down)
        x = jnp.concatenate([before, x, after], axis=dim)
    return x


def rotary_turn(values, places):
    heads = values.shape[1] // HEAD_DIM
    halfway = HEAD_DIM // 2
    quarter = halfway // 2
    column = np.arange(HEAD_DIM)
    swap = np.zeros((HEAD_DIM, HEAD_DIM), np.float32)
    for d in range(HEAD_DIM):
        if d % halfway < quarter:
            swap[d + quarter, d] = -1.0
        else:
            swap[d - quarter, d] = 1.0
    swap = jnp.asarray(np.kron(np.eye(heads, dtype=np.float32), swap), jnp.bfloat16)
    spectrum = ROPE_BASE ** (-jnp.arange(0, halfway, 2, dtype=jnp.float32) / halfway)
    spectrum = jnp.tile(spectrum, values.shape[1] // quarter)
    first_half = jnp.asarray(np.tile(column < halfway, heads))
    offsets = jnp.where(
        first_half[None, :], (places // GRID_W)[:, None], (places % GRID_W)[:, None]
    )
    angles = offsets.astype(jnp.float32) * spectrum[None, :]
    swapped = jnp.dot(values, swap, preferred_element_type=jnp.float32)
    return (values.astype(jnp.float32) * jnp.cos(angles) + swapped * jnp.sin(angles)).astype(
        jnp.bfloat16
    )


def attend_kernel(key_heads, total_rows, first_ref, sink_ref, q_ref, kv_ref, out_ref):
    first = first_ref[0]
    heads = q_ref.shape[1] // HEAD_DIM
    group = heads // key_heads
    shape = (WINDOW, 3 * WINDOW)
    row = lax.broadcasted_iota(jnp.int32, shape, 0)
    column = lax.broadcasted_iota(jnp.int32, shape, 1) - WINDOW
    near = jnp.abs(row - column) <= WINDOW
    for block in range(q_ref.shape[0] // WINDOW):
        start = block * WINDOW
        key_at = column + (first + start)
        allowed = near & (key_at >= 0) & (key_at < total_rows)
        for kh in range(key_heads):
            span = slice(start, start + 3 * WINDOW)
            key = kv_ref[span, kh * HEAD_DIM : (kh + 1) * HEAD_DIM]
            value = kv_ref[span, (key_heads + kh) * HEAD_DIM : (key_heads + kh + 1) * HEAD_DIM]
            for h in range(kh * group, (kh + 1) * group):
                query = q_ref[start : start + WINDOW, h * HEAD_DIM : (h + 1) * HEAD_DIM]
                scores = lax.dot_general(
                    query, key, (((1,), (1,)), ((), ())), preferred_element_type=jnp.float32
                ) * HEAD_DIM ** (-0.5)
                scores = jnp.where(allowed, scores, NEG_LARGE)
                sink = sink_ref[h]
                highest = jnp.maximum(jnp.max(scores, axis=1, keepdims=True), sink)
                lifted = jnp.exp(scores - highest)
                below = jnp.sum(lifted, axis=1, keepdims=True) + jnp.exp(sink - highest)
                chances = (lifted / below).astype(jnp.bfloat16)
                result = jnp.dot(chances, value, preferred_element_type=jnp.float32)
                out_ref[start : start + WINDOW, h * HEAD_DIM : (h + 1) * HEAD_DIM] = result.astype(
                    jnp.bfloat16
                )


def attend(first, sinks, turned, widened, key_heads, total_rows):
    smem = pl.BlockSpec(memory_space=pltpu.SMEM)
    return pl.pallas_call(
        functools.partial(attend_kernel, key_heads, total_rows),
        out_shape=jax.ShapeDtypeStruct(turned.shape, jnp.bfloat16),
        in_specs=[smem, smem, VMEM, VMEM],
        out_specs=VMEM,
        name="attend",
    )(first.reshape(1), sinks, turned, widened)


def places_of(token_split, width_split):
    sp_at = lax.axis_index("sp")
    tp_at = lax.axis_index("tp")
    pair = tp_at + 1 - 2 * (tp_at % 2)
    cross = (tp_at + width_split // 2) % width_split
    return sp_at, tp_at, pair, cross


def flipped(a, b, size):
    total, bit = 0, 1
    while bit < size:
        total = total + (lax.rem(lax.div(a, bit) + lax.div(b, bit), 2)) * bit
        bit *= 2
    return total


def dot32(a, b):
    return jnp.dot(a, b, preferred_element_type=jnp.float32)


def experts_kernel(
    token_split,
    width_split,
    capacity,
    ids_ref,
    weights_ref,
    mixed_ref,
    normed_ref,
    shared_gate_ref,
    shared_up_ref,
    shared_down_ref,
    gate_hbm,
    up_hbm,
    down_hbm,
    out_ref,
    gate_ref,
    up_ref,
    down_ref,
    hidden_ref,
    weigh_ref,
    outgoing,
    arrived,
    from_pair,
    to_cross,
    from_cross,
    back,
    shared_part,
    shared_pair,
    shared_cross,
    shared_got,
    load_sem,
    send,
    recv,
    shared_send,
    shared_recv,
):
    steps, _, rows, width = arrived.shape
    experts = gate_ref.shape[0]
    hid = gate_ref.shape[2]
    own = out_ref.shape[0]
    block_rows = normed_ref.shape[0]
    sp_at, tp_at, pair, cross = places_of(token_split, width_split)
    pair_cross = (pair + width_split // 2) % width_split

    loads = [
        pltpu.make_async_copy(source, target, load_sem.at[n])
        for n, (source, target) in enumerate(
            ((gate_hbm, gate_ref), (up_hbm, up_ref), (down_hbm, down_ref))
        )
    ]
    for load in loads:
        load.start()

    barrier = pltpu.get_barrier_semaphore()

    @pl.loop(1, token_split)
    def _(i):
        pl.semaphore_signal(
            barrier,
            inc=1,
            device_id=(flipped(sp_at, i, token_split), tp_at),
            device_id_type=MESH,
        )

    for partner in (pair, cross):
        pl.semaphore_signal(barrier, inc=1, device_id=(sp_at, partner), device_id_type=MESH)

    square = (block_rows, block_rows)
    before = lax.broadcasted_iota(jnp.int32, square, 0)
    after = lax.broadcasted_iota(jnp.int32, square, 1)
    earlier = (before < after) & (before // own == after // own)
    same_place = before == after
    ids_row = [ids_ref[k : k + 1, :] for k in range(TOPK)]
    ids_column = [
        jnp.sum(jnp.where(same_place, row, 0), axis=1, keepdims=True) for row in ids_row
    ]
    spots = []
    for k in range(TOPK):
        found = jnp.zeros(square, jnp.int32)
        for other in range(TOPK):
            found = found + ((ids_column[other] == ids_row[k]) & earlier).astype(jnp.int32)
        rank = jnp.sum(found, axis=0, keepdims=True)
        home = ids_row[k] // experts
        spots.append(home * rows + (ids_row[k] - home * experts) * capacity + rank)

    def block_spots(b):
        return [spot[:, b * own : (b + 1) * own] for spot in spots]

    own_spots = block_spots(0)
    for b in range(1, width_split):
        own_spots = [jnp.where(tp_at == b, x, y) for x, y in zip(block_spots(b), own_spots)]

    slot_at = lax.broadcasted_iota(jnp.int32, (rows, own), 0)

    def chosen(where_to, at):
        first = at * rows
        return (
            jnp.where(
                (where_to[0] - first == slot_at) | (where_to[1] - first == slot_at), 1.0, 0.0
            )
        ).astype(jnp.bfloat16)

    def remote(stage, i, source, target, where):
        return pltpu.make_async_remote_copy(
            src_ref=source,
            dst_ref=target,
            send_sem=send.at[stage, i],
            recv_sem=recv.at[stage, i],
            device_id=where,
            device_id_type=MESH,
        )

    def partner_of(i):
        return flipped(sp_at, i, token_split)

    def along(i):
        there = partner_of(i)
        return remote(0, i, outgoing.at[there], arrived.at[i, tp_at], (there, tp_at))

    def passed(stage, i, block, partner):
        piece = arrived.at[i, block]
        return remote(stage, i, piece, piece, (sp_at, partner))

    def over(i):
        return passed(1, i, tp_at, cross)

    def beside(i):
        return passed(2, i, tp_at, pair)

    def third(i):
        return passed(3, i, cross, pair)

    def pair_back(side, i):
        block = pair_cross if side == 0 else pair
        return remote(4 + side, i, arrived.at[i, block], from_pair.at[side, i], (sp_at, pair))

    def cross_back(i):
        return remote(6, i, to_cross.at[i], from_cross.at[i], (sp_at, cross))

    def home_copy(i):
        there = partner_of(i)
        return remote(7, i, outgoing.at[there], back.at[sp_at], (there, tp_at))

    def copy_shared(stage, source, target, partner):
        return pltpu.make_async_remote_copy(
            src_ref=source,
            dst_ref=target,
            send_sem=shared_send.at[stage],
            recv_sem=shared_recv.at[stage],
            device_id=(sp_at, partner),
            device_id_type=MESH,
        )

    def shared_side(side):
        block = pair_cross if side == 0 else pair
        return copy_shared(side, shared_part.at[block], shared_pair.at[side], pair)

    shared_over = copy_shared(2, shared_cross, shared_got, cross)

    pl.semaphore_wait(barrier, token_split + 1)

    own_start = pl.multiple_of(tp_at * own, own)

    @pl.loop(1, token_split)
    def _(i):
        there = partner_of(i)
        outgoing[there] = dot32(
            chosen(own_spots, there), normed_ref[pl.ds(own_start, own), :]
        ).astype(outgoing.dtype)
        along(i).start()

    for b in range(width_split):
        arrived[0, b] = dot32(
            chosen(block_spots(b), sp_at), normed_ref[b * own : (b + 1) * own, :]
        ).astype(arrived.dtype)

    for load in loads:
        load.wait()

    row_expert = lax.broadcasted_iota(jnp.int32, (width_split * rows, hid), 0) % rows // capacity
    tile = min(width, 512)

    def silu_times(gate_values, up_values):
        return gate_values / (1.0 + jnp.exp(-gate_values)) * up_values

    def work(i):
        x = arrived[i].reshape(width_split * rows, width)
        for e in range(experts):
            mine = silu_times(dot32(x, gate_ref[e]), dot32(x, up_ref[e]))
            hidden_ref[:, e * hid : (e + 1) * hid] = jnp.where(row_expert == e, mine, 0.0).astype(
                hidden_ref.dtype
            )

        @pl.loop(0, width // tile)
        def _(n):
            at = pl.ds(pl.multiple_of(n * tile, tile), tile)
            result = dot32(hidden_ref[...], down_ref[:, at]).astype(arrived.dtype)
            arrived[i, :, :, at] = result.reshape(width_split, rows, tile)

    def total(*terms):
        value = terms[0].astype(jnp.float32)
        for term in terms[1:]:
            value = value + term.astype(jnp.float32)
        return value

    def forward(i):
        along(i).wait_recv()
        over(i).start()
        beside(i).start()

    def shared_work():
        for b in range(width_split):
            here = normed_ref[b * own : (b + 1) * own, :]
            hidden = silu_times(
                dot32(here, shared_gate_ref[...]), dot32(here, shared_up_ref[...])
            ).astype(jnp.bfloat16)
            shared_part[b] = dot32(hidden, shared_down_ref[...]).astype(shared_part.dtype)
        shared_side(0).start()
        shared_side(1).start()

    def weigh_work():
        square = (own, own)
        eye = lax.broadcasted_iota(jnp.int32, square, 0) == lax.broadcasted_iota(
            jnp.int32, square, 1
        )
        slot_of = lax.broadcasted_iota(jnp.int32, (own, token_split * rows), 1)
        weigh = jnp.zeros((own, token_split * rows), jnp.float32)
        for k in range(TOPK):
            spot = jnp.sum(jnp.where(eye, own_spots[k], 0), axis=1, keepdims=True)
            weight = jnp.sum(
                jnp.where(eye, weights_ref[k : k + 1, :], 0.0), axis=1, keepdims=True
            )
            weigh = jnp.where(slot_of == spot, weight, weigh)
        coarse = weigh.astype(jnp.bfloat16)
        weigh_ref[:own, :] = coarse
        weigh_ref[own:, :] = (weigh - coarse.astype(jnp.float32)).astype(jnp.bfloat16)

    shared_work()

    @pl.loop(0, token_split + 1)
    def _(s):
        @pl.when(s < token_split)
        def _():
            @pl.when(s >= 1)
            def _():
                beside(s).wait()
                third(s).wait()
                over(s).wait_send()

            work(s)
            pair_back(0, s).start()
            pair_back(1, s).start()
            pair_back(0, s).wait_recv()
            to_cross[s] = total(arrived[s, cross], from_pair[0, s]).astype(to_cross.dtype)
            cross_back(s).start()

        @pl.when(s == 0)
        def _():
            shared_side(0).wait_recv()
            shared_cross[...] = total(shared_part[cross], shared_pair[0]).astype(
                shared_cross.dtype
            )
            shared_over.start()
            weigh_work()
            forward(1)

        @pl.when(s + 2 < token_split)
        def _():
            forward(s + 2)

        @pl.when(s + 1 < token_split)
        def _():
            over(s + 1).wait_recv()
            third(s + 1).start()

        @pl.when(s >= 1)
        def _():
            i = s - 1
            pair_back(1, i).wait_recv()
            cross_back(i).wait_recv()
            summed = total(arrived[i, tp_at], from_pair[1, i], from_cross[i]).astype(back.dtype)

            @pl.when(i == 0)
            def _():
                back[sp_at] = summed

            @pl.when(i >= 1)
            def _():
                along(i).wait_send()
                outgoing[partner_of(i)] = summed
                home_copy(i).start()

    shared_side(1).wait_recv()
    shared_over.wait_recv()

    @pl.loop(1, token_split)
    def _(i):
        home_copy(i).wait_recv()

    for n in range(width // tile):
        at = slice(n * tile, (n + 1) * tile)
        routed = dot32(
            weigh_ref[...], back[:, :, at].reshape(token_split * rows, tile)
        )
        out_ref[:, at] = (
            total(
                mixed_ref[pl.ds(own_start, own), at],
                shared_part[tp_at, :, at],
                shared_pair[1, :, at],
                shared_got[:, at],
            )
            + routed[:own]
            + routed[own:]
        ).astype(out_ref.dtype)

    @pl.loop(0, token_split)
    def _(i):
        pair_back(0, i).wait_send()
        pair_back(1, i).wait_send()
        cross_back(i).wait_send()

    @pl.loop(1, token_split)
    def _(i):
        home_copy(i).wait_send()

    shared_side(0).wait_send()
    shared_side(1).wait_send()
    shared_over.wait_send()


def routed_experts(
    ids, weights, mixed, normed, shared_gate, shared_up, shared_down, gate, up, down, sizes
):
    token_split, width_split = sizes
    experts, width, hid = gate.shape
    own = weights.shape[1]
    capacity = max(2, 2 * own * TOPK // (experts * token_split))
    rows = -(-experts * capacity // 16) * 16
    kind = mixed.dtype
    chunk = (rows, width)
    anywhere = pl.BlockSpec(memory_space=pl.ANY)
    return pl.pallas_call(
        functools.partial(experts_kernel, token_split, width_split, capacity),
        out_shape=jax.ShapeDtypeStruct((own, width), kind),
        in_specs=[VMEM] * 7 + [anywhere] * 3,
        out_specs=VMEM,
        scratch_shapes=[
            pltpu.VMEM(gate.shape, kind),
            pltpu.VMEM(up.shape, kind),
            pltpu.VMEM((experts * hid, width), kind),
            pltpu.VMEM((width_split * rows, experts * hid), kind),
            pltpu.VMEM((2 * own, token_split * rows), kind),
            pltpu.VMEM((token_split,) + chunk, kind),
            pltpu.VMEM((token_split, width_split) + chunk, kind),
            pltpu.VMEM((2, token_split) + chunk, kind),
            pltpu.VMEM((token_split,) + chunk, kind),
            pltpu.VMEM((token_split,) + chunk, kind),
            pltpu.VMEM((token_split,) + chunk, kind),
            pltpu.VMEM((width_split, own, width), kind),
            pltpu.VMEM((2, own, width), kind),
            pltpu.VMEM((own, width), kind),
            pltpu.VMEM((own, width), kind),
            pltpu.SemaphoreType.DMA((3,)),
            pltpu.SemaphoreType.DMA((8, token_split)),
            pltpu.SemaphoreType.DMA((8, token_split)),
            pltpu.SemaphoreType.DMA((3,)),
            pltpu.SemaphoreType.DMA((3,)),
        ],
        compiler_params=pltpu.CompilerParams(
            collective_id=1, has_side_effects=True, vmem_limit_bytes=VMEM_LIMIT
        ),
        name="experts",
    )(
        ids,
        weights,
        mixed,
        normed,
        shared_gate,
        shared_up,
        shared_down,
        gate,
        up,
        down.reshape(experts * hid, width),
    )


def per_device(
    queries,
    keys,
    values,
    sinks,
    residual,
    out_weight,
    norm_gain,
    shared_gate,
    shared_up,
    shared_down,
    expert_ids,
    route_weights,
    expert_gate,
    expert_up,
    expert_down,
):
    block_rows = queries.shape[0]
    width_split = lax.axis_size("tp")
    token_split = lax.axis_size("sp")
    width_index = lax.axis_index("tp")
    key_heads = keys.shape[1] // HEAD_DIM
    heads_local = queries.shape[1] // HEAD_DIM
    first_row = lax.axis_index("sp") * block_rows
    total_rows = token_split * block_rows
    places = first_row + jnp.arange(block_rows, dtype=jnp.int32)
    turned = rotary_turn(jnp.concatenate([queries, keys], axis=1), places)
    query_width = heads_local * HEAD_DIM
    joined = jnp.concatenate([turned[:, query_width:], values], axis=1)
    widened = extended(joined, (("sp", 0),), WINDOW)
    attended = attend(
        first_row, sinks, turned[:, :query_width], widened, key_heads, total_rows
    )
    model_width = out_weight.shape[1]
    projected = jnp.dot(
        lax.all_gather(attended, "tp", axis=1, tiled=True),
        out_weight,
        preferred_element_type=jnp.float32,
    )
    mixed_rows = (residual.astype(jnp.float32) + projected).astype(jnp.bfloat16)
    mixed_float = mixed_rows.astype(jnp.float32)
    scale_rows = lax.rsqrt(
        jnp.mean(mixed_float * mixed_float, axis=-1, keepdims=True) + NORM_EPSILON
    )
    normed = (mixed_float * scale_rows * norm_gain).astype(jnp.bfloat16)
    return routed_experts(
        expert_ids.T,
        route_weights.T,
        mixed_rows,
        normed,
        shared_gate,
        shared_up,
        shared_down,
        expert_gate,
        expert_up,
        expert_down,
        (token_split, width_split),
    )


def solution(mesh):
    placed = (
        P("sp", "tp"),
        P("sp", "tp"),
        P("sp", "tp"),
        P("tp"),
        P("sp", None),
        P(),
        P(),
        P(None, "tp"),
        P(None, "tp"),
        P("tp", None),
        P("sp", None),
        P(("sp", "tp"), None),
        P("sp", None, "tp"),
        P("sp", None, "tp"),
        P("sp", "tp", None),
    )
    return jax.shard_map(
        per_device, mesh=mesh, in_specs=placed, out_specs=P(("sp", "tp"), None), check_vma=False
    )
```

time: 185 us -> 150 us (0.81)
  the two profiles are of different devices: /device:TPU:0 before, /device:TPU:9 now
where the time goes in v1:
time: 150 us
  Pallas kernels  115 us (77%)
  blocking collectives  9.5 us (6%)
  local copies, waits for them, and re-layouts  7.87 us (5%)
  matrix products  7.01 us (5%)
  starting transfers between devices  6.18 us (4%)
  other arithmetic  2.48 us (2%)
  waiting for transfers between devices  1.58 us (1%)
    pallas_call x1, Pallas kernels, routed_experts(): pl.pallas_call(functools.partial(experts_kernel, token_split, width_split...  110 us
    all_gather x1, blocking collectives, per_device(): lax.all_gather(attended, 'tp', axis=1, tiled=True)  9.5 us
    unnamed x12, local copies, waits for them, and re-layouts  6.63 us
    pallas_call x1, Pallas kernels, attend(): pl.pallas_call(functools.partial(attend_kernel, key_heads, total_rows), o...  5 us
    dot_general x2, matrix products, rotary_turn(): swapped = jnp.dot(values, swap, preferred_element_type=jnp.float32)  3.88 us
    dot_general x1, matrix products, per_device(): jnp.dot(lax.all_gather(attended, 'tp', axis=1, tiled=True), out_weight, p...  3.12 us
    ppermute x1, starting transfers between devices, extended(): before = lax.ppermute(last, axis, up)  3.12 us
    ppermute x1, starting transfers between devices, extended(): after = lax.ppermute(initial, axis, down)  3.06 us
  transfers between devices with their start and end apart: 2, of which 1 were waited for; matrix products, arithmetic and copies ran while one was open for 0% of the time, Pallas kernels for 0%

profile of v1, /device:TPU:9, one launch (start us, length us, event | category | flops | bytes accessed | tf_op | source)
XLA Modules:
  0.0 149.9 jit_solution(14698076137770745206)
XLA Ops:
  0.0 0.0 copy-start
  0.0 0.1 mul.47
  0.1 1.1 copy.27
  1.2 0.9 copy.24
  2.1 1.7 %copy.23 = bf16[384,192]{1,0:T(8,128)(2,1)} copy(bf16[384,192]{0,1:T(8,128)(2,1)} %param.17) | data formatting | bytes 294912 | tf_op args[0]
  3.8 1.2 fusion.10
  5.1 2.7 %fusion.6 = bf16[384,256]{1,0:T(8,128)(2,1)S(1)} fusion(f32[256,384]{0,1:T(8,128)S(1)} %fusion.10, bf16[64,256]{1,0:T(8,128)(2,1)} %constant.61, bf16[384,64]{0,1:T(8,128)(2,1)} %param.18, bf16[384,64]{1,0:T(8,128)(2,1)S(1)} %copy.24, bf16[384,192]{1,0:T(8,128)(2,1)} %copy.23, f32[256]{0:T(256)S(1)} %mul.47, s32[384]{0:T(512)S(1)} %get-tuple-element.9, ...), kind=kOutput, calls=%fused_computation.10 | convolution fusion | flops 13762560 | bytes 872704 | tf_op jit(solution)/shard_map/dot_general | solution.py:57
  7.7 0.0 copy-start.2
  7.8 0.1 slice.19
  7.9 0.1 pad_maximum_fusion.2
  8.0 3.1 %collective-permute-start = (bf16[128,128]{1,0:T(8,128)(2,1)S(1)}, bf16[128,128]{1,0:T(8,128)(2,1)S(1)}, u32[]{:S(2)}, u32[]{:S(2)}) collective-permute-start(bf16[128,128]{1,0:T(8,128)(2,1)S(1)} %get-tuple-element.5), channel_id=1, source_target_pairs={{0,4},{4,8},{8,12},{12,16},{16,20},{20,24},{24,28},{1,5},{5,9},{9,... | collective-permute-start | bytes 98312 | tf_op jit(solution)/shard_map/ppermute | solution.py:32
  11.1 3.1 %collective-permute-start.1 = (bf16[128,128]{1,0:T(8,128)(2,1)S(1)}, bf16[128,128]{1,0:T(8,128)(2,1)S(1)}, u32[]{:S(2)}, u32[]{:S(2)}) collective-permute-start(bf16[128,128]{1,0:T(8,128)(2,1)S(1)} %get-tuple-element.6), channel_id=1, source_target_pairs={{4,0},{8,4},{12,8},{16,12},{20,16},{24,20},{28,24},{5,1},{9,5},{13... | collective-permute-start | bytes 98312 | tf_op jit(solution)/shard_map/ppermute | solution.py:33
  14.1 0.0 collective-permute-done
  14.2 1.6 %collective-permute-done.1 = bf16[128,128]{1,0:T(8,128)(2,1)S(1)} collective-permute-done((bf16[128,128]{1,0:T(8,128)(2,1)S(1)}, bf16[128,128]{1,0:T(8,128)(2,1)S(1)}, u32[]{:S(2)}, u32[]{:S(2)}) %collective-permute-start.1) | collective-permute-done | bytes 32800 | tf_op jit(solution)/shard_map/ppermute | solution.py:33
  15.7 0.8 pad_maximum_fusion.kv_ref
  16.5 0.0 copy-done.2
  16.5 5.0 %attend.1 = bf16[384,192]{1,0:T(8,128)(2,1)} custom-call(s32[1]{0:T(128)} %bitcast.2.first_ref, f32[3]{0:T(128)} %sink_ref.1, bf16[384,192]{1,0:T(8,128)(2,1)} %bitcast.20, bf16[640,128]{1,0:T(8,128)(2,1)} %pad_maximum_fusion.kv_ref), custom_call_target="tpu_custom_call" | custom-call | tf_op jit(solution)/shard_map/attend/pallas_call | solution.py:98
  21.5 1.1 copy.28
  22.6 9.5 %all_gather.3 = bf16[384,768]{0,1:T(8,128)(2,1)S(1)} all-gather(bf16[384,192]{0,1:T(8,128)(2,1)S(1)} %copy.28), channel_id=1, replica_groups=mesh['sp'=8,'tp'=4] {'tp'}, dimensions={1}, use_global_device_ids=true | all-gather | bytes 737280 | tf_op jit(solution)/shard_map/all_gather | solution.py:548
  32.1 0.0 copy-done
  32.1 0.0 copy-start.3
  32.1 3.1 %fusion = (f32[384]{0:T(512)S(1)}, bf16[384,2048]{1,0:T(8,128)(2,1)S(1)}) fusion(bf16[384,768]{0,1:T(8,128)(2,1)S(1)} %all_gather.3, bf16[768,2048]{1,0:T(8,128)(2,1)S(1)} %copy-done, bf16[384,2048]{1,0:T(8,128)(2,1)} %param.21), kind=kOutput, calls=%fused_computation.2 | convolution fusion | flops 1212677760 | bytes 6882816 | tf_op jit(solution)/shard_map/dot_general | solution.py:547
  35.2 0.0 copy-start.1
  35.2 1.1 copy-done.1
  36.4 0.0 copy-done.3
  36.4 1.6 %fusion.2.normed_ref = bf16[384,2048]{1,0:T(8,128)(2,1)} fusion(bf16[384,2048]{1,0:T(8,128)(2,1)S(1)} %get-tuple-element.8.mixed_ref, f32[2048]{0:T(1024)S(1)} %copy-done.3, f32[384]{0:T(512)S(1)} %add_rsqrt_fusion), kind=kLoop, calls=%fused_computation.4 | loop fusion | flops 3145728 | bytes 3155456 | tf_op jit(solution)/shard_map/convert_element_type | solution.py:557
  38.0 110.2 %experts.1 = bf16[96,2048]{1,0:T(8,128)(2,1)} custom-call(s32[2,384]{1,0:T(2,128)} %bitcast.21, f32[2,96]{1,0:T(2,128)} %bitcast.22, bf16[384,2048]{1,0:T(8,128)(2,1)} %copy-done.1, bf16[384,2048]{1,0:T(8,128)(2,1)} %fusion.2.normed_ref, bf16[2048,128]{1,0:T(8,128)(2,1)} %shared_gate_ref.1, bf16[2048,128]{1,0:T(8,128)(2,1)} %shared_up_ref.1, ...), custom_call_target="tpu_custom_call" | custom-call | tf_op jit(solution)/shard_map/experts/pallas_call | solution.py:468
  148.1 1.8 %copy.32 = bf16[96,2048]{1,0:T(8,128)(2,1)} copy(bf16[96,2048]{1,0:T(8,128)(2,1)} %experts.1) | data formatting | bytes 786432
  (4 shorter events, 0.0 us)
Async XLA Ops:
  0.0 32.1 %copy-start = (bf16[768,2048]{1,0:T(8,128)(2,1)S(1)}, bf16[768,2048]{1,0:T(8,128)(2,1)}, u32[]{:S(2)}) copy-start(bf16[768,2048]{1,0:T(8,128)(2,1)} %param.22) | copy-start | bytes 9437188
  7.7 8.8 %copy-start.2 = (bf16[384,256]{1,0:T(8,128)(2,1)}, bf16[384,256]{1,0:T(8,128)(2,1)S(1)}, u32[]{:S(2)}) copy-start(bf16[384,256]{1,0:T(8,128)(2,1)S(1)} %fusion.6) | copy-start | bytes 589828
  8.0 6.2 %collective-permute-start = (bf16[128,128]{1,0:T(8,128)(2,1)S(1)}, bf16[128,128]{1,0:T(8,128)(2,1)S(1)}, u32[]{:S(2)}, u32[]{:S(2)}) collective-permute-start(bf16[128,128]{1,0:T(8,128)(2,1)S(1)} %get-tuple-element.5), channel_id=1, source_target_pairs={{0,4},{4,8},{8,12},{12,16},{16,20},{20,24},{24,28},{1,5},{5,9},{9,... | collective-permute-start | bytes 98312 | tf_op jit(solution)/shard_map/ppermute | solution.py:32
  11.1 4.7 %collective-permute-start.1 = (bf16[128,128]{1,0:T(8,128)(2,1)S(1)}, bf16[128,128]{1,0:T(8,128)(2,1)S(1)}, u32[]{:S(2)}, u32[]{:S(2)}) collective-permute-start(bf16[128,128]{1,0:T(8,128)(2,1)S(1)} %get-tuple-element.6), channel_id=1, source_target_pairs={{4,0},{8,4},{12,8},{16,12},{20,16},{24,20},{28,24},{5,1},{9,5},{13... | collective-permute-start | bytes 98312 | tf_op jit(solution)/shard_map/ppermute | solution.py:33
  32.1 4.3 %copy-start.3 = (f32[2048]{0:T(1024)S(1)}, f32[2048]{0:T(1024)}, u32[]{:S(2)}) copy-start(f32[2048]{0:T(1024)} %param.23) | copy-start | bytes 24580
  35.2 1.2 copy-start.1

commit v2 on v1

--- a/solution.py
+++ b/solution.py
@@ -104,14 +104,6 @@
     )(first.reshape(1), sinks, turned, widened)
 
 
-def places_of(token_split, width_split):
-    sp_at = lax.axis_index("sp")
-    tp_at = lax.axis_index("tp")
-    pair = tp_at + 1 - 2 * (tp_at % 2)
-    cross = (tp_at + width_split // 2) % width_split
-    return sp_at, tp_at, pair, cross
-
-
 def flipped(a, b, size):
     total, bit = 0, 1
     while bit < size:
@@ -124,55 +116,94 @@
     return jnp.dot(a, b, preferred_element_type=jnp.float32)
 
 
+def total(*terms):
+    value = terms[0].astype(jnp.float32)
+    for term in terms[1:]:
+        value = value + term.astype(jnp.float32)
+    return value
+
+
+def silu_times(gate_values, up_values):
+    return gate_values / (1.0 + jnp.exp(-gate_values)) * up_values
+
+
 def experts_kernel(
     token_split,
-    width_split,
     capacity,
     ids_ref,
     weights_ref,
     mixed_ref,
     normed_ref,
-    shared_gate_ref,
-    shared_up_ref,
-    shared_down_ref,
+    shared_gate_hbm,
+    shared_up_hbm,
+    shared_down_hbm,
     gate_hbm,
     up_hbm,
     down_hbm,
     out_ref,
-    gate_ref,
-    up_ref,
-    down_ref,
-    hidden_ref,
+    shared_gate,
+    shared_up,
+    shared_down,
+    gate,
+    up,
+    down,
+    column_rows,
+    hidden,
     weigh_ref,
     outgoing,
+    outgoing_other,
     arrived,
-    from_pair,
-    to_cross,
+    part,
     from_cross,
     back,
     shared_part,
-    shared_pair,
-    shared_cross,
     shared_got,
     load_sem,
+    weight_send,
+    weight_recv,
     send,
     recv,
-    shared_send,
-    shared_recv,
+    shared_sem,
 ):
-    steps, _, rows, width = arrived.shape
-    experts = gate_ref.shape[0]
-    hid = gate_ref.shape[2]
+    _, experts, rows, width = arrived.shape
+    hid = gate.shape[3]
+    shared_hid = shared_down_hbm.shape[0]
     own = out_ref.shape[0]
     block_rows = normed_ref.shape[0]
-    sp_at, tp_at, pair, cross = places_of(token_split, width_split)
-    pair_cross = (pair + width_split // 2) % width_split
+    halves = experts
+    sp_at = lax.axis_index("sp")
+    tp_at = lax.axis_index("tp")
+    column = lax.rem(tp_at, 2)
+    half = lax.div(tp_at, 2)
+    other = 1 - half
+    pair = 2 * half + 1 - column
+    cross = 2 * other + column
+
+    def weight_pairs(which):
+        side = pl.ds(which * shared_hid, shared_hid)
+        return (
+            (shared_gate_hbm, shared_gate.at[:, side]),
+            (shared_up_hbm, shared_up.at[:, side]),
+            (shared_down_hbm, shared_down.at[side, :]),
+            (gate_hbm, gate.at[which]),
+            (up_hbm, up.at[which]),
+            (down_hbm, down.at[:, pl.ds(which * hid, hid), :]),
+        )
 
     loads = [
         pltpu.make_async_copy(source, target, load_sem.at[n])
-        for n, (source, target) in enumerate(
-            ((gate_hbm, gate_ref), (up_hbm, up_ref), (down_hbm, down_ref))
+        for n, (source, target) in enumerate(weight_pairs(0))
+    ]
+    shares = [
+        pltpu.make_async_remote_copy(
+            src_ref=source,
+            dst_ref=target,
+            send_sem=weight_send.at[n],
+            recv_sem=weight_recv.at[n],
+            device_id=(sp_at, pair),
+            device_id_type=MESH,
         )
+        for n, (source, target) in enumerate(weight_pairs(1))
     ]
     for load in loads:
         load.start()
@@ -200,31 +231,40 @@
     ids_column = [
         jnp.sum(jnp.where(same_place, row, 0), axis=1, keepdims=True) for row in ids_row
     ]
-    spots = []
+    half_row = lax.broadcasted_iota(jnp.int32, (1, block_rows), 1) // (2 * own)
+    codes, spots = [], []
     for k in range(TOPK):
         found = jnp.zeros(square, jnp.int32)
-        for other in range(TOPK):
-            found = found + ((ids_column[other] == ids_row[k]) & earlier).astype(jnp.int32)
+        for another in range(TOPK):
+            found = found + ((ids_column[another] == ids_row[k]) & earlier).astype(jnp.int32)
         rank = jnp.sum(found, axis=0, keepdims=True)
         home = ids_row[k] // experts
         spots.append(home * rows + (ids_row[k] - home * experts) * capacity + rank)
-
-    def block_spots(b):
-        return [spot[:, b * own : (b + 1) * own] for spot in spots]
-
-    own_spots = block_spots(0)
-    for b in range(1, width_split):
-        own_spots = [jnp.where(tp_at == b, x, y) for x, y in zip(block_spots(b), own_spots)]
-
-    slot_at = lax.broadcasted_iota(jnp.int32, (rows, own), 0)
-
-    def chosen(where_to, at):
-        first = at * rows
-        return (
-            jnp.where(
-                (where_to[0] - first == slot_at) | (where_to[1] - first == slot_at), 1.0, 0.0
-            )
+        codes.append(ids_row[k] * rows + half_row * capacity + rank)
+
+    def block_of(row, b):
+        return row[:, b * own : (b + 1) * own]
+
+    def column_block(row, b):
+        return jnp.where(column == 0, block_of(row, 2 * b), block_of(row, 2 * b + 1))
+
+    column_codes = [
+        jnp.concatenate([column_block(code, b) for b in range(halves)], axis=1) for code in codes
+    ]
+    own_spots = [
+        jnp.where(half == 0, column_block(spot, 0), column_block(spot, 1)) for spot in spots
+    ]
+    slot_at = lax.broadcasted_iota(jnp.int32, (rows, halves * own), 0)
+
+    def chosen(at, expert):
+        wanted = slot_at + (at * experts + expert) * rows
+        return jnp.where(
+            (column_codes[0] == wanted) | (column_codes[1] == wanted), 1.0, 0.0
         ).astype(jnp.bfloat16)
+
+    for b in range(halves):
+        start = pl.multiple_of((2 * b + column) * own, own)
+        column_rows[b * own : (b + 1) * own, :] = normed_ref[pl.ds(start, own), :]
 
     def remote(stage, i, source, target, where):
         return pltpu.make_async_remote_copy(
@@ -239,110 +279,103 @@
     def partner_of(i):
         return flipped(sp_at, i, token_split)
 
+    near = token_split // 2
+    middle = lax.rem(lax.div(sp_at, near) + lax.div(sp_at, max(1, near // 2)), 2)
+
+    def in_order(step):
+        return flipped(step, middle * (near // 2) * lax.div(step, near), token_split)
+
     def along(i):
         there = partner_of(i)
-        return remote(0, i, outgoing.at[there], arrived.at[i, tp_at], (there, tp_at))
-
-    def passed(stage, i, block, partner):
-        piece = arrived.at[i, block]
-        return remote(stage, i, piece, piece, (sp_at, partner))
+        return remote(0, i, outgoing.at[there], arrived.at[i, half], (there, tp_at))
+
+    def along_other(i):
+        there = partner_of(i)
+        return remote(1, i, outgoing_other.at[i], arrived.at[i, other], (there, tp_at))
 
     def over(i):
-        return passed(1, i, tp_at, cross)
-
-    def beside(i):
-        return passed(2, i, tp_at, pair)
-
-    def third(i):
-        return passed(3, i, cross, pair)
-
-    def pair_back(side, i):
-        block = pair_cross if side == 0 else pair
-        return remote(4 + side, i, arrived.at[i, block], from_pair.at[side, i], (sp_at, pair))
+        piece = arrived.at[i, half]
+        return remote(1, i, piece, piece, (sp_at, cross))
 
     def cross_back(i):
-        return remote(6, i, to_cross.at[i], from_cross.at[i], (sp_at, cross))
+        return remote(2, i, part.at[i, other], from_cross.at[i], (sp_at, cross))
 
     def home_copy(i):
         there = partner_of(i)
-        return remote(7, i, outgoing.at[there], back.at[sp_at], (there, tp_at))
-
-    def copy_shared(stage, source, target, partner):
-        return pltpu.make_async_remote_copy(
-            src_ref=source,
-            dst_ref=target,
-            send_sem=shared_send.at[stage],
-            recv_sem=shared_recv.at[stage],
-            device_id=(sp_at, partner),
-            device_id_type=MESH,
-        )
-
-    def shared_side(side):
-        block = pair_cross if side == 0 else pair
-        return copy_shared(side, shared_part.at[block], shared_pair.at[side], pair)
-
-    shared_over = copy_shared(2, shared_cross, shared_got, cross)
+        return remote(3, i, outgoing.at[there], back.at[sp_at], (there, tp_at))
+
+    shared_over = pltpu.make_async_remote_copy(
+        src_ref=shared_part.at[other],
+        dst_ref=shared_got,
+        send_sem=shared_sem.at[0],
+        recv_sem=shared_sem.at[1],
+        device_id=(sp_at, cross),
+        device_id_type=MESH,
+    )
 
     pl.semaphore_wait(barrier, token_split + 1)
 
-    own_start = pl.multiple_of(tp_at * own, own)
+    for share in shares:
+        share.start()
 
     @pl.loop(1, token_split)
-    def _(i):
+    def _(step):
+        i = 1 + lax.rem(step - 1 + middle * (near - 1), token_split - 1)
         there = partner_of(i)
-        outgoing[there] = dot32(
-            chosen(own_spots, there), normed_ref[pl.ds(own_start, own), :]
-        ).astype(outgoing.dtype)
+        outgoing[there] = dot32(chosen(there, half), column_rows[...]).astype(outgoing.dtype)
         along(i).start()
 
-    for b in range(width_split):
-        arrived[0, b] = dot32(
-            chosen(block_spots(b), sp_at), normed_ref[b * own : (b + 1) * own, :]
-        ).astype(arrived.dtype)
-
-    for load in loads:
-        load.wait()
-
-    row_expert = lax.broadcasted_iota(jnp.int32, (width_split * rows, hid), 0) % rows // capacity
+        @pl.when(i < near)
+        def _():
+            outgoing_other[i] = dot32(chosen(there, other), column_rows[...]).astype(
+                outgoing_other.dtype
+            )
+            along_other(i).start()
+
+    for e in range(experts):
+        arrived[0, e] = dot32(chosen(sp_at, e), column_rows[...]).astype(arrived.dtype)
+
     tile = min(width, 512)
 
-    def silu_times(gate_values, up_values):
-        return gate_values / (1.0 + jnp.exp(-gate_values)) * up_values
-
     def work(i):
-        x = arrived[i].reshape(width_split * rows, width)
         for e in range(experts):
-            mine = silu_times(dot32(x, gate_ref[e]), dot32(x, up_ref[e]))
-            hidden_ref[:, e * hid : (e + 1) * hid] = jnp.where(row_expert == e, mine, 0.0).astype(
-                hidden_ref.dtype
-            )
+            x = arrived[i, e]
+            for p in range(2):
+                hidden[e, :, p * hid : (p + 1) * hid] = silu_times(
+                    dot32(x, gate[p, e]), dot32(x, up[p, e])
+                ).astype(hidden.dtype)
 
         @pl.loop(0, width // tile)
         def _(n):
             at = pl.ds(pl.multiple_of(n * tile, tile), tile)
-            result = dot32(hidden_ref[...], down_ref[:, at]).astype(arrived.dtype)
-            arrived[i, :, :, at] = result.reshape(width_split, rows, tile)
-
-    def total(*terms):
-        value = terms[0].astype(jnp.float32)
-        for term in terms[1:]:
-            value = value + term.astype(jnp.float32)
-        return value
-
-    def forward(i):
+            results = [dot32(hidden[e], down[e, :, at]) for e in range(experts)]
+            for b in range(halves):
+                if capacity % 8 == 0 and rows == experts * capacity:
+                    piece = jnp.concatenate(
+                        [result[b * capacity : (b + 1) * capacity] for result in results], axis=0
+                    )
+                else:
+                    piece = jnp.zeros((rows, tile), jnp.float32)
+                    into = lax.broadcasted_iota(jnp.int32, (rows, rows), 0)
+                    source = lax.broadcasted_iota(jnp.int32, (rows, rows), 1)
+                    for e in range(experts):
+                        rank = into - e * capacity
+                        picked = (
+                            (rank >= 0) & (rank < capacity) & (source == rank + b * capacity)
+                        )
+                        piece = piece + dot32(
+                            jnp.where(picked, 1.0, 0.0).astype(jnp.bfloat16),
+                            results[e].astype(jnp.bfloat16),
+                        )
+                part[i, b, :, at] = piece.astype(part.dtype)
+
+    def forward(step):
+        i = in_order(step)
         along(i).wait_recv()
-        over(i).start()
-        beside(i).start()
-
-    def shared_work():
-        for b in range(width_split):
-            here = normed_ref[b * own : (b + 1) * own, :]
-            hidden = silu_times(
-                dot32(here, shared_gate_ref[...]), dot32(here, shared_up_ref[...])
-            ).astype(jnp.bfloat16)
-            shared_part[b] = dot32(hidden, shared_down_ref[...]).astype(shared_part.dtype)
-        shared_side(0).start()
-        shared_side(1).start()
+
+        @pl.when(step >= near)
+        def _():
+            over(i).start()
 
     def weigh_work():
         square = (own, own)
@@ -361,79 +394,75 @@
         weigh_ref[:own, :] = coarse
         weigh_ref[own:, :] = (weigh - coarse.astype(jnp.float32)).astype(jnp.bfloat16)
 
-    shared_work()
+    for n in range(3):
+        loads[n].wait()
+        shares[n].wait()
+    shared_hidden = silu_times(
+        dot32(column_rows[...], shared_gate[...]), dot32(column_rows[...], shared_up[...])
+    ).astype(jnp.bfloat16)
+    for n in range(width // tile):
+        at = slice(n * tile, (n + 1) * tile)
+        shared_part[:, :, at] = (
+            dot32(shared_hidden, shared_down[:, at])
+            .astype(shared_part.dtype)
+            .reshape(halves, own, tile)
+        )
+    shared_over.start()
+    weigh_work()
+    for n in range(3, 6):
+        loads[n].wait()
+        shares[n].wait()
 
     @pl.loop(0, token_split + 1)
-    def _(s):
-        @pl.when(s < token_split)
+    def _(step):
+        @pl.when(step < token_split)
         def _():
-            @pl.when(s >= 1)
+            i = in_order(step)
+
+            @pl.when(step >= 1)
             def _():
-                beside(s).wait()
-                third(s).wait()
-                over(s).wait_send()
-
-            work(s)
-            pair_back(0, s).start()
-            pair_back(1, s).start()
-            pair_back(0, s).wait_recv()
-            to_cross[s] = total(arrived[s, cross], from_pair[0, s]).astype(to_cross.dtype)
-            cross_back(s).start()
-
-        @pl.when(s == 0)
+                over(i).wait_recv()
+
+            work(i)
+            cross_back(i).start()
+
+        @pl.when(step == 0)
         def _():
-            shared_side(0).wait_recv()
-            shared_cross[...] = total(shared_part[cross], shared_pair[0]).astype(
-                shared_cross.dtype
-            )
-            shared_over.start()
-            weigh_work()
             forward(1)
 
-        @pl.when(s + 2 < token_split)
+        @pl.when(step >= 1)
         def _():
-            forward(s + 2)
-
-        @pl.when(s + 1 < token_split)
-        def _():
-            over(s + 1).wait_recv()
-            third(s + 1).start()
-
-        @pl.when(s >= 1)
-        def _():
-            i = s - 1
-            pair_back(1, i).wait_recv()
+            i = in_order(step - 1)
             cross_back(i).wait_recv()
-            summed = total(arrived[i, tp_at], from_pair[1, i], from_cross[i]).astype(back.dtype)
-
-            @pl.when(i == 0)
+            summed = total(part[i, half], from_cross[i]).astype(back.dtype)
+
+            @pl.when(step == 1)
             def _():
                 back[sp_at] = summed
 
-            @pl.when(i >= 1)
+            @pl.when(step >= 2)
             def _():
                 along(i).wait_send()
                 outgoing[partner_of(i)] = summed
                 home_copy(i).start()
 
-    shared_side(1).wait_recv()
+        @pl.when(step + 2 < token_split)
+        def _():
+            forward(step + 2)
+
     shared_over.wait_recv()
 
     @pl.loop(1, token_split)
     def _(i):
         home_copy(i).wait_recv()
 
+    own_start = pl.multiple_of(tp_at * own, own)
     for n in range(width // tile):
         at = slice(n * tile, (n + 1) * tile)
-        routed = dot32(
-            weigh_ref[...], back[:, :, at].reshape(token_split * rows, tile)
-        )
+        routed = dot32(weigh_ref[...], back[:, :, at].reshape(token_split * rows, tile))
         out_ref[:, at] = (
             total(
-                mixed_ref[pl.ds(own_start, own), at],
-                shared_part[tp_at, :, at],
-                shared_pair[1, :, at],
-                shared_got[:, at],
+                mixed_ref[pl.ds(own_start, own), at], shared_part[half, :, at], shared_got[:, at]
             )
             + routed[:own]
             + routed[own:]
@@ -441,16 +470,13 @@
 
     @pl.loop(0, token_split)
     def _(i):
-        pair_back(0, i).wait_send()
-        pair_back(1, i).wait_send()
         cross_back(i).wait_send()
 
     @pl.loop(1, token_split)
     def _(i):
+        over(i).wait_send()
         home_copy(i).wait_send()
 
-    shared_side(0).wait_send()
-    shared_side(1).wait_send()
     shared_over.wait_send()
 
 
@@ -459,55 +485,51 @@
 ):
     token_split, width_split = sizes
     experts, width, hid = gate.shape
+    if experts != 2 or width_split != 4:
+        raise ValueError("unsupported split")
     own = weights.shape[1]
     capacity = max(2, 2 * own * TOPK // (experts * token_split))
     rows = -(-experts * capacity // 16) * 16
+    shared_hid = shared_gate.shape[1]
     kind = mixed.dtype
     chunk = (rows, width)
-    anywhere = pl.BlockSpec(memory_space=pl.ANY)
+    hbm = pl.BlockSpec(memory_space=pltpu.HBM)
+    dma = pltpu.SemaphoreType.DMA
     return pl.pallas_call(
-        functools.partial(experts_kernel, token_split, width_split, capacity),
+        functools.partial(experts_kernel, token_split, capacity),
         out_shape=jax.ShapeDtypeStruct((own, width), kind),
-        in_specs=[VMEM] * 7 + [anywhere] * 3,
+        in_specs=[VMEM] * 4 + [hbm] * 6,
         out_specs=VMEM,
         scratch_shapes=[
-            pltpu.VMEM(gate.shape, kind),
-            pltpu.VMEM(up.shape, kind),
-            pltpu.VMEM((experts * hid, width), kind),
-            pltpu.VMEM((width_split * rows, experts * hid), kind),
+            pltpu.VMEM((width, 2 * shared_hid), kind),
+            pltpu.VMEM((width, 2 * shared_hid), kind),
+            pltpu.VMEM((2 * shared_hid, width), kind),
+            pltpu.VMEM((2, experts, width, hid), kind),
+            pltpu.VMEM((2, experts, width, hid), kind),
+            pltpu.VMEM((experts, 2 * hid, width), kind),
+            pltpu.VMEM((2 * own, width), kind),
+            pltpu.VMEM((experts, rows, 2 * hid), kind),
             pltpu.VMEM((2 * own, token_split * rows), kind),
             pltpu.VMEM((token_split,) + chunk, kind),
-            pltpu.VMEM((token_split, width_split) + chunk, kind),
-            pltpu.VMEM((2, token_split) + chunk, kind),
+            pltpu.VMEM((token_split // 2,) + chunk, kind),
+            pltpu.VMEM((token_split, experts) + chunk, kind),
+            pltpu.VMEM((token_split, 2) + chunk, kind),
             pltpu.VMEM((token_split,) + chunk, kind),
             pltpu.VMEM((token_split,) + chunk, kind),
-            pltpu.VMEM((token_split,) + chunk, kind),
-            pltpu.VMEM((width_split, own, width), kind),
             pltpu.VMEM((2, own, width), kind),
             pltpu.VMEM((own, width), kind),
-            pltpu.VMEM((own, width), kind),
-            pltpu.SemaphoreType.DMA((3,)),
-            pltpu.SemaphoreType.DMA((8, token_split)),
-            pltpu.SemaphoreType.DMA((8, token_split)),
-            pltpu.SemaphoreType.DMA((3,)),
-            pltpu.SemaphoreType.DMA((3,)),
+            dma((6,)),
+            dma((6,)),
+            dma((6,)),
+            dma((4, token_split)),
+            dma((4, token_split)),
+            dma((2,)),
         ],
         compiler_params=pltpu.CompilerParams(
             collective_id=1, has_side_effects=True, vmem_limit_bytes=VMEM_LIMIT
         ),
         name="experts",
-    )(
-        ids,
-        weights,
-        mixed,
-        normed,
-        shared_gate,
-        shared_up,
-        shared_down,
-        gate,
-        up,
-        down.reshape(experts * hid, width),
-    )
+    )(ids, weights, mixed, normed, shared_gate, shared_up, shared_down, gate, up, down)
 
 
 def per_device(

time: 150 us -> 132 us (0.88)
  the two profiles are of different devices: /device:TPU:9 before, /device:TPU:0 now
where the time goes in v2:
time: 132 us
  Pallas kernels  95.8 us (73%)
  local copies, waits for them, and re-layouts  7.87 us (6%)
  blocking collectives  7.56 us (6%)
  matrix products  7.01 us (5%)
  starting transfers between devices  6.16 us (5%)
  waiting for transfers between devices  4.51 us (3%)
  other arithmetic  2.48 us (2%)
    pallas_call x1, Pallas kernels, routed_experts(): pl.pallas_call(functools.partial(experts_kernel, token_split, capacity),...  90.8 us
    all_gather x1, blocking collectives, per_device(): lax.all_gather(attended, 'tp', axis=1, tiled=True)  7.56 us
    unnamed x12, local copies, waits for them, and re-layouts  6.63 us
    pallas_call x1, Pallas kernels, attend(): pl.pallas_call(functools.partial(attend_kernel, key_heads, total_rows), o...  5 us
    ppermute x1, starting transfers between devices, extended(): before = lax.ppermute(last, axis, up)  4.87 us
    ppermute x1, waiting for transfers between devices, extended(): after = lax.ppermute(initial, axis, down)  4.23 us
    dot_general x2, matrix products, rotary_turn(): swapped = jnp.dot(values, swap, preferred_element_type=jnp.float32)  3.88 us
    dot_general x1, matrix products, per_device(): jnp.dot(lax.all_gather(attended, 'tp', axis=1, tiled=True), out_weight, p...  3.12 us
  transfers between devices with their start and end apart: 2, of which 2 were waited for; matrix products, arithmetic and copies ran while one was open for 0% of the time, Pallas kernels for 0%

profile of v2, /device:TPU:0, one launch (start us, length us, event | category | flops | bytes accessed | tf_op | source)
XLA Modules:
  0.0 131.5 jit_solution(1867458073328158935)
XLA Ops:
  0.0 0.0 copy-start
  0.0 0.1 mul.47
  0.1 1.1 copy.27
  1.2 0.9 copy.24
  2.1 1.7 %copy.23 = bf16[384,192]{1,0:T(8,128)(2,1)} copy(bf16[384,192]{0,1:T(8,128)(2,1)} %param.17) | data formatting | bytes 294912 | tf_op args[0]
  3.8 1.2 fusion.10
  5.1 2.7 %fusion.6 = bf16[384,256]{1,0:T(8,128)(2,1)S(1)} fusion(f32[256,384]{0,1:T(8,128)S(1)} %fusion.10, bf16[64,256]{1,0:T(8,128)(2,1)} %constant.61, bf16[384,64]{0,1:T(8,128)(2,1)} %param.18, bf16[384,64]{1,0:T(8,128)(2,1)S(1)} %copy.24, bf16[384,192]{1,0:T(8,128)(2,1)} %copy.23, f32[256]{0:T(256)S(1)} %mul.47, s32[384]{0:T(512)S(1)} %get-tuple-element.9, ...), kind=kOutput, calls=%fused_computation.10 | convolution fusion | flops 13762560 | bytes 872704 | tf_op jit(solution)/shard_map/dot_general | solution.py:57
  7.7 0.0 copy-start.2
  7.8 0.1 slice.19
  7.9 0.1 pad_maximum_fusion.2
  8.0 4.9 %collective-permute-start = (bf16[128,128]{1,0:T(8,128)(2,1)S(1)}, bf16[128,128]{1,0:T(8,128)(2,1)S(1)}, u32[]{:S(2)}, u32[]{:S(2)}) collective-permute-start(bf16[128,128]{1,0:T(8,128)(2,1)S(1)} %get-tuple-element.5), channel_id=1, source_target_pairs={{0,4},{4,8},{8,12},{12,16},{16,20},{20,24},{24,28},{1,5},{5,9},{9,... | collective-permute-start | bytes 98312 | tf_op jit(solution)/shard_map/ppermute | solution.py:32
  12.8 1.3 collective-permute-start.1
  14.1 0.3 collective-permute-done
  14.4 4.2 %collective-permute-done.1 = bf16[128,128]{1,0:T(8,128)(2,1)S(1)} collective-permute-done((bf16[128,128]{1,0:T(8,128)(2,1)S(1)}, bf16[128,128]{1,0:T(8,128)(2,1)S(1)}, u32[]{:S(2)}, u32[]{:S(2)}) %collective-permute-start.1) | collective-permute-done | bytes 32800 | tf_op jit(solution)/shard_map/ppermute | solution.py:33
  18.6 0.8 pad_maximum_fusion.kv_ref
  19.4 0.0 copy-done.2
  19.4 5.0 %attend.1 = bf16[384,192]{1,0:T(8,128)(2,1)} custom-call(s32[1]{0:T(128)} %bitcast.2.first_ref, f32[3]{0:T(128)} %sink_ref.1, bf16[384,192]{1,0:T(8,128)(2,1)} %bitcast.18, bf16[640,128]{1,0:T(8,128)(2,1)} %pad_maximum_fusion.kv_ref), custom_call_target="tpu_custom_call" | custom-call | tf_op jit(solution)/shard_map/attend/pallas_call | solution.py:98
  24.4 1.1 copy.28
  25.5 7.6 %all_gather.3 = bf16[384,768]{0,1:T(8,128)(2,1)S(1)} all-gather(bf16[384,192]{0,1:T(8,128)(2,1)S(1)} %copy.28), channel_id=1, replica_groups=mesh['sp'=8,'tp'=4] {'tp'}, dimensions={1}, use_global_device_ids=true | all-gather | bytes 737280 | tf_op jit(solution)/shard_map/all_gather | solution.py:570
  33.0 0.0 copy-done
  33.0 0.0 copy-start.3
  33.0 3.1 %fusion = (f32[384]{0:T(512)S(1)}, bf16[384,2048]{1,0:T(8,128)(2,1)S(1)}) fusion(bf16[384,768]{0,1:T(8,128)(2,1)S(1)} %all_gather.3, bf16[768,2048]{1,0:T(8,128)(2,1)S(1)} %copy-done, bf16[384,2048]{1,0:T(8,128)(2,1)} %param.21), kind=kOutput, calls=%fused_computation.2 | convolution fusion | flops 1212677760 | bytes 6882816 | tf_op jit(solution)/shard_map/dot_general | solution.py:569
  36.2 0.0 copy-start.1
  36.2 1.1 copy-done.1
  37.3 0.0 copy-done.3
  37.3 1.6 %fusion.2.normed_ref = bf16[384,2048]{1,0:T(8,128)(2,1)} fusion(bf16[384,2048]{1,0:T(8,128)(2,1)S(1)} %get-tuple-element.8.mixed_ref, f32[2048]{0:T(1024)S(1)} %copy-done.3, f32[384]{0:T(512)S(1)} %add_rsqrt_fusion), kind=kLoop, calls=%fused_computation.4 | loop fusion | flops 3145728 | bytes 3155456 | tf_op jit(solution)/shard_map/convert_element_type | solution.py:579
  38.9 90.8 %experts.1 = bf16[96,2048]{1,0:T(8,128)(2,1)} custom-call(s32[2,384]{1,0:T(2,128)} %bitcast.19, f32[2,96]{1,0:T(2,128)} %bitcast.20, bf16[384,2048]{1,0:T(8,128)(2,1)} %copy-done.1, bf16[384,2048]{1,0:T(8,128)(2,1)} %fusion.2.normed_ref, bf16[2048,128]{1,0:T(8,128)(2,1)} %shared_gate_hbm.1, bf16[2048,128]{1,0:T(8,128)(2,1)} %shared_up_hbm.1, ...), custom_call_target="tpu_custom_call" | custom-call | tf_op jit(solution)/shard_map/experts/pallas_call | solution.py:498
  129.7 1.8 %copy.32 = bf16[96,2048]{1,0:T(8,128)(2,1)} copy(bf16[96,2048]{1,0:T(8,128)(2,1)} %experts.1) | data formatting | bytes 786432
  (4 shorter events, 0.0 us)
Async XLA Ops:
  0.0 33.0 %copy-start = (bf16[768,2048]{1,0:T(8,128)(2,1)S(1)}, bf16[768,2048]{1,0:T(8,128)(2,1)}, u32[]{:S(2)}) copy-start(bf16[768,2048]{1,0:T(8,128)(2,1)} %param.22) | copy-start | bytes 9437188
  7.7 11.7 %copy-start.2 = (bf16[384,256]{1,0:T(8,128)(2,1)}, bf16[384,256]{1,0:T(8,128)(2,1)S(1)}, u32[]{:S(2)}) copy-start(bf16[384,256]{1,0:T(8,128)(2,1)S(1)} %fusion.6) | copy-start | bytes 589828
  8.0 6.5 %collective-permute-start = (bf16[128,128]{1,0:T(8,128)(2,1)S(1)}, bf16[128,128]{1,0:T(8,128)(2,1)S(1)}, u32[]{:S(2)}, u32[]{:S(2)}) collective-permute-start(bf16[128,128]{1,0:T(8,128)(2,1)S(1)} %get-tuple-element.5), channel_id=1, source_target_pairs={{0,4},{4,8},{8,12},{12,16},{16,20},{20,24},{24,28},{1,5},{5,9},{9,... | collective-permute-start | bytes 98312 | tf_op jit(solution)/shard_map/ppermute | solution.py:32
  12.8 5.8 %collective-permute-start.1 = (bf16[128,128]{1,0:T(8,128)(2,1)S(1)}, bf16[128,128]{1,0:T(8,128)(2,1)S(1)}, u32[]{:S(2)}, u32[]{:S(2)}) collective-permute-start(bf16[128,128]{1,0:T(8,128)(2,1)S(1)} %get-tuple-element.6), channel_id=1, source_target_pairs={{4,0},{8,4},{12,8},{16,12},{20,16},{24,20},{28,24},{5,1},{9,5},{13... | collective-permute-start | bytes 98312 | tf_op jit(solution)/shard_map/ppermute | solution.py:33
  33.0 4.3 %copy-start.3 = (f32[2048]{0:T(1024)S(1)}, f32[2048]{0:T(1024)}, u32[]{:S(2)}) copy-start(f32[2048]{0:T(1024)} %param.23) | copy-start | bytes 24580
  36.2 1.2 copy-start.1

commit v3 on v2

--- a/solution.py
+++ b/solution.py
@@ -9,7 +9,7 @@
 
 MESH = pl.DeviceIdType.MESH
 VMEM = pl.BlockSpec(memory_space=pltpu.VMEM)
-VMEM_LIMIT = 60 * 1024 * 1024
+VMEM_LIMIT = 62 * 1024 * 1024
 
 HEAD_DIM = 64
 WINDOW = 128
@@ -22,86 +22,17 @@
 NORM_EPSILON = 1e-06
 
 
-def extended(x, sides, width):
-    for axis, dim in sides:
-        size, length = (lax.axis_size(axis), x.shape[dim])
-        up = [(i, (i + 1) % size) for i in range(size - 1)]
-        down = [(j, i) for i, j in up]
-        last = lax.slice_in_dim(x, length - width, length, axis=dim)
-        initial = lax.slice_in_dim(x, 0, width, axis=dim)
-        before = lax.ppermute(last, axis, up)
-        after = lax.ppermute(initial, axis, down)
-        x = jnp.concatenate([before, x, after], axis=dim)
-    return x
-
-
-def rotary_turn(values, places):
-    heads = values.shape[1] // HEAD_DIM
+def turn_tables(total_rows):
     halfway = HEAD_DIM // 2
-    quarter = halfway // 2
-    column = np.arange(HEAD_DIM)
-    swap = np.zeros((HEAD_DIM, HEAD_DIM), np.float32)
-    for d in range(HEAD_DIM):
-        if d % halfway < quarter:
-            swap[d + quarter, d] = -1.0
-        else:
-            swap[d - quarter, d] = 1.0
-    swap = jnp.asarray(np.kron(np.eye(heads, dtype=np.float32), swap), jnp.bfloat16)
-    spectrum = ROPE_BASE ** (-jnp.arange(0, halfway, 2, dtype=jnp.float32) / halfway)
-    spectrum = jnp.tile(spectrum, values.shape[1] // quarter)
-    first_half = jnp.asarray(np.tile(column < halfway, heads))
-    offsets = jnp.where(
-        first_half[None, :], (places // GRID_W)[:, None], (places % GRID_W)[:, None]
+    spectrum = np.float32(ROPE_BASE) ** (
+        -np.arange(0, halfway, 2, dtype=np.float32) / np.float32(halfway)
     )
-    angles = offsets.astype(jnp.float32) * spectrum[None, :]
-    swapped = jnp.dot(values, swap, preferred_element_type=jnp.float32)
-    return (values.astype(jnp.float32) * jnp.cos(angles) + swapped * jnp.sin(angles)).astype(
-        jnp.bfloat16
-    )
-
-
-def attend_kernel(key_heads, total_rows, first_ref, sink_ref, q_ref, kv_ref, out_ref):
-    first = first_ref[0]
-    heads = q_ref.shape[1] // HEAD_DIM
-    group = heads // key_heads
-    shape = (WINDOW, 3 * WINDOW)
-    row = lax.broadcasted_iota(jnp.int32, shape, 0)
-    column = lax.broadcasted_iota(jnp.int32, shape, 1) - WINDOW
-    near = jnp.abs(row - column) <= WINDOW
-    for block in range(q_ref.shape[0] // WINDOW):
-        start = block * WINDOW
-        key_at = column + (first + start)
-        allowed = near & (key_at >= 0) & (key_at < total_rows)
-        for kh in range(key_heads):
-            span = slice(start, start + 3 * WINDOW)
-            key = kv_ref[span, kh * HEAD_DIM : (kh + 1) * HEAD_DIM]
-            value = kv_ref[span, (key_heads + kh) * HEAD_DIM : (key_heads + kh + 1) * HEAD_DIM]
-            for h in range(kh * group, (kh + 1) * group):
-                query = q_ref[start : start + WINDOW, h * HEAD_DIM : (h + 1) * HEAD_DIM]
-                scores = lax.dot_general(
-                    query, key, (((1,), (1,)), ((), ())), preferred_element_type=jnp.float32
-                ) * HEAD_DIM ** (-0.5)
-                scores = jnp.where(allowed, scores, NEG_LARGE)
-                sink = sink_ref[h]
-                highest = jnp.maximum(jnp.max(scores, axis=1, keepdims=True), sink)
-                lifted = jnp.exp(scores - highest)
-                below = jnp.sum(lifted, axis=1, keepdims=True) + jnp.exp(sink - highest)
-                chances = (lifted / below).astype(jnp.bfloat16)
-                result = jnp.dot(chances, value, preferred_element_type=jnp.float32)
-                out_ref[start : start + WINDOW, h * HEAD_DIM : (h + 1) * HEAD_DIM] = result.astype(
-                    jnp.bfloat16
-                )
-
-
-def attend(first, sinks, turned, widened, key_heads, total_rows):
-    smem = pl.BlockSpec(memory_space=pltpu.SMEM)
-    return pl.pallas_call(
-        functools.partial(attend_kernel, key_heads, total_rows),
-        out_shape=jax.ShapeDtypeStruct(turned.shape, jnp.bfloat16),
-        in_specs=[smem, smem, VMEM, VMEM],
-        out_specs=VMEM,
-        name="attend",
-    )(first.reshape(1), sinks, turned, widened)
+    places = np.arange(total_rows)
+    tables = []
+    for offsets in (places // GRID_W, places % GRID_W):
+        angles = spectrum[:, None].astype(np.float32) * offsets.astype(np.float32)[None, :]
+        tables += [np.cos(angles), np.sin(angles)]
+    return np.stack(tables).astype(np.float32)
 
 
 def flipped(a, b, size):
@@ -127,13 +58,19 @@
     return gate_values / (1.0 + jnp.exp(-gate_values)) * up_values
 
 
-def experts_kernel(
+def layer_kernel(
     token_split,
     capacity,
+    sinks_ref,
+    queries_ref,
+    keys_ref,
+    values_ref,
+    gain_ref,
     ids_ref,
     weights_ref,
-    mixed_ref,
-    normed_ref,
+    tables_hbm,
+    residual_hbm,
+    out_weight_hbm,
     shared_gate_hbm,
     shared_up_hbm,
     shared_down_hbm,
@@ -141,6 +78,16 @@
     up_hbm,
     down_hbm,
     out_ref,
+    tables,
+    residual,
+    out_weight,
+    turned,
+    near_keys,
+    near_values,
+    attended,
+    gathered,
+    summed_rows,
+    mixed,
     shared_gate,
     shared_up,
     shared_down,
@@ -164,12 +111,17 @@
     send,
     recv,
     shared_sem,
+    first_sem,
+    halo_send,
+    halo_recv,
+    gather_send,
+    gather_recv,
 ):
     _, experts, rows, width = arrived.shape
     hid = gate.shape[3]
     shared_hid = shared_down_hbm.shape[0]
     own = out_ref.shape[0]
-    block_rows = normed_ref.shape[0]
+    block_rows = queries_ref.shape[1]
     halves = experts
     sp_at = lax.axis_index("sp")
     tp_at = lax.axis_index("tp")
@@ -178,6 +130,7 @@
     other = 1 - half
     pair = 2 * half + 1 - column
     cross = 2 * other + column
+    diagonal = 2 * other + 1 - column
 
     def weight_pairs(which):
         side = pl.ds(which * shared_hid, shared_hid)
@@ -205,8 +158,38 @@
         )
         for n, (source, target) in enumerate(weight_pairs(1))
     ]
-    for load in loads:
+    def column_start(b):
+        return pl.multiple_of((2 * b + column) * own, own)
+
+    first_row = pl.multiple_of(sp_at * block_rows, block_rows)
+    first_loads = [
+        pltpu.make_async_copy(source, target, first_sem.at[n])
+        for n, (source, target) in enumerate(
+            [
+                (tables_hbm.at[:, :, pl.ds(first_row, block_rows)], tables),
+                (out_weight_hbm, out_weight),
+            ]
+            + [
+                (residual_hbm.at[pl.ds(column_start(b), own)], residual.at[b])
+                for b in range(halves)
+            ]
+        )
+    ]
+    for load in first_loads + loads:
         load.start()
+
+    group_width, _ = queries_ref.shape
+    group = group_width // HEAD_DIM
+
+    @pl.when(sp_at == 0)
+    def _():
+        near_keys[:WINDOW, :] = jnp.zeros((WINDOW, HEAD_DIM), near_keys.dtype)
+        near_values[:, :WINDOW] = jnp.zeros((HEAD_DIM, WINDOW), near_values.dtype)
+
+    @pl.when(sp_at == token_split - 1)
+    def _():
+        near_keys[WINDOW + block_rows :, :] = jnp.zeros((WINDOW, HEAD_DIM), near_keys.dtype)
+        near_values[:, WINDOW + block_rows :] = jnp.zeros((HEAD_DIM, WINDOW), near_values.dtype)
 
     barrier = pltpu.get_barrier_semaphore()
 
@@ -219,8 +202,67 @@
             device_id_type=MESH,
         )
 
-    for partner in (pair, cross):
+    for partner in (pair, cross, diagonal):
         pl.semaphore_signal(barrier, inc=1, device_id=(sp_at, partner), device_id_type=MESH)
+
+    first_loads[0].wait()
+    quarter = HEAD_DIM // 4
+
+    def turn(ref, base):
+        pieces = []
+        for n in range(2):
+            cosine, sine = tables[2 * n], tables[2 * n + 1]
+            start = base + 2 * n * quarter
+            former = ref[start : start + quarter, :].astype(jnp.float32)
+            latter = ref[start + quarter : start + 2 * quarter, :].astype(jnp.float32)
+            pieces += [former * cosine - latter * sine, former * sine + latter * cosine]
+        return pieces
+
+    turned_keys = jnp.concatenate(turn(keys_ref, 0), axis=0)
+    near_keys[WINDOW : WINDOW + block_rows, :] = turned_keys.T.astype(near_keys.dtype)
+    near_values[:, WINDOW : WINDOW + block_rows] = values_ref[...]
+    pl.semaphore_wait(barrier, token_split + 2)
+
+    def halo(n, direction):
+        lo = WINDOW if direction == 0 else block_rows
+        to = WINDOW + block_rows if direction == 0 else 0
+        there = sp_at - 1 if direction == 0 else sp_at + 1
+        if n == 0:
+            source, target = near_keys.at[lo : lo + WINDOW, :], near_keys.at[to : to + WINDOW, :]
+        else:
+            source, target = (
+                near_values.at[:, lo : lo + WINDOW],
+                near_values.at[:, to : to + WINDOW],
+            )
+        return pltpu.make_async_remote_copy(
+            src_ref=source,
+            dst_ref=target,
+            send_sem=halo_send.at[direction, n],
+            recv_sem=halo_recv.at[direction, n],
+            device_id=(there, tp_at),
+            device_id_type=MESH,
+        )
+
+    has_before = sp_at > 0
+    has_after = sp_at < token_split - 1
+
+    @pl.when(has_before)
+    def _():
+        halo(0, 0).start()
+        halo(1, 0).start()
+
+    @pl.when(has_after)
+    def _():
+        halo(0, 1).start()
+        halo(1, 1).start()
+
+    for share in shares[:4]:
+        share.start()
+
+    for h in range(group):
+        for n, piece in enumerate(turn(queries_ref, h * HEAD_DIM)):
+            start = h * HEAD_DIM + n * quarter
+            turned[start : start + quarter, :] = piece.astype(turned.dtype)
 
     square = (block_rows, block_rows)
     before = lax.broadcasted_iota(jnp.int32, square, 0)
@@ -262,10 +304,6 @@
             (column_codes[0] == wanted) | (column_codes[1] == wanted), 1.0, 0.0
         ).astype(jnp.bfloat16)
 
-    for b in range(halves):
-        start = pl.multiple_of((2 * b + column) * own, own)
-        column_rows[b * own : (b + 1) * own, :] = normed_ref[pl.ds(start, own), :]
-
     def remote(stage, i, source, target, where):
         return pltpu.make_async_remote_copy(
             src_ref=source,
@@ -313,10 +351,135 @@
         device_id_type=MESH,
     )
 
-    pl.semaphore_wait(barrier, token_split + 1)
-
-    for share in shares:
+    def weigh_work():
+        square = (own, own)
+        eye = lax.broadcasted_iota(jnp.int32, square, 0) == lax.broadcasted_iota(
+            jnp.int32, square, 1
+        )
+        slot_of = lax.broadcasted_iota(jnp.int32, (own, token_split * rows), 1)
+        weigh = jnp.zeros((own, token_split * rows), jnp.float32)
+        for k in range(TOPK):
+            spot = jnp.sum(jnp.where(eye, own_spots[k], 0), axis=1, keepdims=True)
+            weight = jnp.sum(
+                jnp.where(eye, weights_ref[k : k + 1, :], 0.0), axis=1, keepdims=True
+            )
+            weigh = jnp.where(slot_of == spot, weight, weigh)
+        coarse = weigh.astype(jnp.bfloat16)
+        weigh_ref[:own, :] = coarse
+        weigh_ref[own:, :] = (weigh - coarse.astype(jnp.float32)).astype(jnp.bfloat16)
+
+    weigh_work()
+
+    key_at = lax.broadcasted_iota(jnp.int32, (3 * WINDOW, group * WINDOW), 0)
+    query_at = lax.broadcasted_iota(jnp.int32, (3 * WINDOW, group * WINDOW), 1)
+    near_enough = jnp.abs(key_at - WINDOW - query_at % WINDOW) <= WINDOW
+    head_at = lax.broadcasted_iota(jnp.int32, (1, group * WINDOW), 1) // WINDOW
+    sink = jnp.full((1, group * WINDOW), sinks_ref[0])
+    for h in range(1, group):
+        sink = jnp.where(head_at == h, sinks_ref[h], sink)
+    blocks = block_rows // WINDOW
+    total_rows = token_split * block_rows
+
+    def attend(block):
+        start = block * WINDOW
+        query = jnp.concatenate(
+            [
+                turned[h * HEAD_DIM : (h + 1) * HEAD_DIM, start : start + WINDOW]
+                for h in range(group)
+            ],
+            axis=1,
+        )
+        allowed = near_enough
+        if block == 0:
+            allowed = allowed & (key_at + (first_row - WINDOW) >= 0)
+        if block == blocks - 1:
+            allowed = allowed & (key_at + (first_row + start - WINDOW) < total_rows)
+        scores = dot32(near_keys[start : start + 3 * WINDOW, :], query) * HEAD_DIM ** (-0.5)
+        scores = jnp.where(allowed, scores, NEG_LARGE)
+        highest = jnp.maximum(jnp.max(scores, axis=0, keepdims=True), sink)
+        lifted = jnp.exp(scores - highest)
+        below = jnp.sum(lifted, axis=0, keepdims=True) + jnp.exp(sink - highest)
+        chances = (lifted * (1.0 / below)).astype(jnp.bfloat16)
+        result = dot32(near_values[:, start : start + 3 * WINDOW], chances)
+        heads = jnp.concatenate(
+            [result[:, h * WINDOW : (h + 1) * WINDOW] for h in range(group)], axis=0
+        )
+        attended[start : start + WINDOW, :] = heads.T.astype(attended.dtype)
+
+    for block in range(1, blocks - 1):
+        attend(block)
+
+    @pl.when(has_before)
+    def _():
+        halo(0, 1).wait_recv()
+        halo(1, 1).wait_recv()
+
+    attend(0)
+
+    @pl.when(has_after)
+    def _():
+        halo(0, 0).wait_recv()
+        halo(1, 0).wait_recv()
+
+    if blocks > 1:
+        attend(blocks - 1)
+
+    def gather(n, b):
+        partner = (cross, diagonal, pair)[n]
+        start = pl.multiple_of((2 * b + lax.rem(partner, 2)) * own, own)
+        return pltpu.make_async_remote_copy(
+            src_ref=attended.at[pl.ds(start, own), :],
+            dst_ref=gathered.at[tp_at, b],
+            send_sem=gather_send.at[n, b],
+            recv_sem=gather_recv.at[n, b],
+            device_id=(sp_at, partner),
+            device_id_type=MESH,
+        )
+
+    for n in range(3):
+        for b in range(halves):
+            gather(n, b).start()
+    for b in range(halves):
+        gathered[tp_at, b] = attended[pl.ds(column_start(b), own), :]
+    for share in shares[4:]:
         share.start()
+    for load in first_loads[1:]:
+        load.wait()
+
+    tile = min(width, 512)
+
+    def projected(source, at):
+        rows_at = pl.ds(pl.multiple_of(source * group_width, group_width), group_width)
+        return dot32(
+            gathered[source].reshape(halves * own, group_width), out_weight[rows_at, at]
+        )
+
+    @pl.loop(0, width // tile)
+    def _(n):
+        at = pl.ds(pl.multiple_of(n * tile, tile), tile)
+        summed_rows[:, at] = projected(tp_at, at) + residual[:, :, at].reshape(
+            halves * own, tile
+        ).astype(jnp.float32)
+
+    for n in range(3):
+        for b in range(halves):
+            gather(n, b).wait_recv()
+
+    squares = jnp.zeros((halves * own, 1), jnp.float32)
+    for n in range(width // tile):
+        at = slice(n * tile, (n + 1) * tile)
+        value = summed_rows[:, at]
+        for source in (pair, cross, diagonal):
+            value = value + projected(source, at)
+        value = value.astype(mixed.dtype)
+        mixed[:, :, at] = value.reshape(halves, own, tile)
+        value = value.astype(jnp.float32)
+        squares = squares + jnp.sum(value * value, axis=1, keepdims=True)
+    scale_rows = lax.rsqrt(squares * (1.0 / width) + NORM_EPSILON)
+    for n in range(width // tile):
+        at = slice(n * tile, (n + 1) * tile)
+        value = mixed[:, :, at].reshape(halves * own, tile).astype(jnp.float32)
+        column_rows[:, at] = (value * scale_rows * gain_ref[:, at]).astype(column_rows.dtype)
 
     @pl.loop(1, token_split)
     def _(step):
@@ -334,8 +497,6 @@
 
     for e in range(experts):
         arrived[0, e] = dot32(chosen(sp_at, e), column_rows[...]).astype(arrived.dtype)
-
-    tile = min(width, 512)
 
     def work(i):
         for e in range(experts):
@@ -377,23 +538,6 @@
         def _():
             over(i).start()
 
-    def weigh_work():
-        square = (own, own)
-        eye = lax.broadcasted_iota(jnp.int32, square, 0) == lax.broadcasted_iota(
-            jnp.int32, square, 1
-        )
-        slot_of = lax.broadcasted_iota(jnp.int32, (own, token_split * rows), 1)
-        weigh = jnp.zeros((own, token_split * rows), jnp.float32)
-        for k in range(TOPK):
-            spot = jnp.sum(jnp.where(eye, own_spots[k], 0), axis=1, keepdims=True)
-            weight = jnp.sum(
-                jnp.where(eye, weights_ref[k : k + 1, :], 0.0), axis=1, keepdims=True
-            )
-            weigh = jnp.where(slot_of == spot, weight, weigh)
-        coarse = weigh.astype(jnp.bfloat16)
-        weigh_ref[:own, :] = coarse
-        weigh_ref[own:, :] = (weigh - coarse.astype(jnp.float32)).astype(jnp.bfloat16)
-
     for n in range(3):
         loads[n].wait()
         shares[n].wait()
@@ -408,7 +552,6 @@
             .reshape(halves, own, tile)
         )
     shared_over.start()
-    weigh_work()
     for n in range(3, 6):
         loads[n].wait()
         shares[n].wait()
@@ -456,14 +599,11 @@
     def _(i):
         home_copy(i).wait_recv()
 
-    own_start = pl.multiple_of(tp_at * own, own)
     for n in range(width // tile):
         at = slice(n * tile, (n + 1) * tile)
         routed = dot32(weigh_ref[...], back[:, :, at].reshape(token_split * rows, tile))
         out_ref[:, at] = (
-            total(
-                mixed_ref[pl.ds(own_start, own), at], shared_part[half, :, at], shared_got[:, at]
-            )
+            total(mixed[half, :, at], shared_part[half, :, at], shared_got[:, at])
             + routed[:own]
             + routed[own:]
         ).astype(out_ref.dtype)
@@ -478,29 +618,69 @@
         home_copy(i).wait_send()
 
     shared_over.wait_send()
-
-
-def routed_experts(
-    ids, weights, mixed, normed, shared_gate, shared_up, shared_down, gate, up, down, sizes
+    for n in range(3):
+        for b in range(halves):
+            gather(n, b).wait_send()
+
+    @pl.when(has_before)
+    def _():
+        halo(0, 0).wait_send()
+        halo(1, 0).wait_send()
+
+    @pl.when(has_after)
+    def _():
+        halo(0, 1).wait_send()
+        halo(1, 1).wait_send()
+
+
+def per_device(
+    queries,
+    keys,
+    values,
+    sinks,
+    residual,
+    out_weight,
+    norm_gain,
+    shared_gate,
+    shared_up,
+    shared_down,
+    expert_ids,
+    route_weights,
+    expert_gate,
+    expert_up,
+    expert_down,
 ):
-    token_split, width_split = sizes
-    experts, width, hid = gate.shape
-    if experts != 2 or width_split != 4:
+    token_split = lax.axis_size("sp")
+    width_split = lax.axis_size("tp")
+    experts, width, hid = expert_gate.shape
+    block_rows, query_width = queries.shape
+    if experts != 2 or width_split != 4 or keys.shape[1] != HEAD_DIM:
         raise ValueError("unsupported split")
-    own = weights.shape[1]
+    own = route_weights.shape[0]
     capacity = max(2, 2 * own * TOPK // (experts * token_split))
     rows = -(-experts * capacity // 16) * 16
     shared_hid = shared_gate.shape[1]
-    kind = mixed.dtype
+    kind = queries.dtype
     chunk = (rows, width)
     hbm = pl.BlockSpec(memory_space=pltpu.HBM)
     dma = pltpu.SemaphoreType.DMA
+    wide_rows = block_rows + 2 * WINDOW
     return pl.pallas_call(
-        functools.partial(experts_kernel, token_split, capacity),
+        functools.partial(layer_kernel, token_split, capacity),
         out_shape=jax.ShapeDtypeStruct((own, width), kind),
-        in_specs=[VMEM] * 4 + [hbm] * 6,
+        in_specs=[pl.BlockSpec(memory_space=pltpu.SMEM)] + [VMEM] * 6 + [hbm] * 9,
         out_specs=VMEM,
         scratch_shapes=[
+            pltpu.VMEM((4, HEAD_DIM // 4, block_rows), jnp.float32),
+            pltpu.VMEM((2, own, width), kind),
+            pltpu.VMEM(out_weight.shape, kind),
+            pltpu.VMEM((query_width, block_rows), kind),
+            pltpu.VMEM((wide_rows, HEAD_DIM), kind),
+            pltpu.VMEM((HEAD_DIM, wide_rows), kind),
+            pltpu.VMEM((block_rows, query_width), kind),
+            pltpu.VMEM((width_split, 2, own, query_width), kind),
+            pltpu.VMEM((2 * own, width), jnp.float32),
+            pltpu.VMEM((2, own, width), kind),
             pltpu.VMEM((width, 2 * shared_hid), kind),
             pltpu.VMEM((width, 2 * shared_hid), kind),
             pltpu.VMEM((2 * shared_hid, width), kind),
@@ -524,71 +704,33 @@
             dma((4, token_split)),
             dma((4, token_split)),
             dma((2,)),
+            dma((4,)),
+            dma((2, 2)),
+            dma((2, 2)),
+            dma((3, 2)),
+            dma((3, 2)),
         ],
         compiler_params=pltpu.CompilerParams(
             collective_id=1, has_side_effects=True, vmem_limit_bytes=VMEM_LIMIT
         ),
-        name="experts",
-    )(ids, weights, mixed, normed, shared_gate, shared_up, shared_down, gate, up, down)
-
-
-def per_device(
-    queries,
-    keys,
-    values,
-    sinks,
-    residual,
-    out_weight,
-    norm_gain,
-    shared_gate,
-    shared_up,
-    shared_down,
-    expert_ids,
-    route_weights,
-    expert_gate,
-    expert_up,
-    expert_down,
-):
-    block_rows = queries.shape[0]
-    width_split = lax.axis_size("tp")
-    token_split = lax.axis_size("sp")
-    width_index = lax.axis_index("tp")
-    key_heads = keys.shape[1] // HEAD_DIM
-    heads_local = queries.shape[1] // HEAD_DIM
-    first_row = lax.axis_index("sp") * block_rows
-    total_rows = token_split * block_rows
-    places = first_row + jnp.arange(block_rows, dtype=jnp.int32)
-    turned = rotary_turn(jnp.concatenate([queries, keys], axis=1), places)
-    query_width = heads_local * HEAD_DIM
-    joined = jnp.concatenate([turned[:, query_width:], values], axis=1)
-    widened = extended(joined, (("sp", 0),), WINDOW)
-    attended = attend(
-        first_row, sinks, turned[:, :query_width], widened, key_heads, total_rows
-    )
-    model_width = out_weight.shape[1]
-    projected = jnp.dot(
-        lax.all_gather(attended, "tp", axis=1, tiled=True),
-        out_weight,
-        preferred_element_type=jnp.float32,
-    )
-    mixed_rows = (residual.astype(jnp.float32) + projected).astype(jnp.bfloat16)
-    mixed_float = mixed_rows.astype(jnp.float32)
-    scale_rows = lax.rsqrt(
-        jnp.mean(mixed_float * mixed_float, axis=-1, keepdims=True) + NORM_EPSILON
-    )
-    normed = (mixed_float * scale_rows * norm_gain).astype(jnp.bfloat16)
-    return routed_experts(
+        name="layer",
+    )(
+        sinks,
+        queries.T,
+        keys.T,
+        values.T,
+        norm_gain.reshape(1, width),
         expert_ids.T,
         route_weights.T,
-        mixed_rows,
-        normed,
+        jnp.asarray(turn_tables(token_split * block_rows)),
+        residual,
+        out_weight,
         shared_gate,
         shared_up,
         shared_down,
         expert_gate,
         expert_up,
         expert_down,
-        (token_split, width_split),
     )
 
 

time: 132 us -> 106 us (0.80)
  the two profiles are of different devices: /device:TPU:0 before, /device:TPU:3 now
where the time goes in v3:
time: 106 us
  Pallas kernels  104 us (98%)
  local copies, waits for them, and re-layouts  1.77 us (2%)
    pallas_call x1, Pallas kernels, per_device(): pl.pallas_call(functools.partial(layer_kernel, token_split, capacity), ou...  104 us

profile of v3, /device:TPU:3, one launch (start us, length us, event | category | flops | bytes accessed | tf_op | source)
XLA Modules:
  0.0 106.2 jit_solution(16371237043909518176)
XLA Ops:
  0.0 104.4 %layer.1 = bf16[96,2048]{1,0:T(8,128)(2,1)} custom-call(f32[3]{0:T(128)} %sinks_ref.1, bf16[192,384]{1,0:T(8,128)(2,1)} %bitcast.6, bf16[64,384]{1,0:T(8,128)(2,1)} %bitcast.7, bf16[64,384]{1,0:T(8,128)(2,1)} %bitcast.8, f32[1,2048]{1,0:T(1,128)} %bitcast.9, s32[2,384]{1,0:T(2,128)} %bitcast.10, f32[2,96]{1,0:T(2,128)} %bitcast.11, ...), custom_call_target="tpu_custom_call" | custom-call | tf_op jit(solution)/shard_map/layer/pallas_call | solution.py:668
  104.4 1.8 %copy.18 = bf16[96,2048]{1,0:T(8,128)(2,1)} copy(bf16[96,2048]{1,0:T(8,128)(2,1)} %layer.1) | data formatting | bytes 786432

commit v4 on v3

--- a/solution.py
+++ b/solution.py
@@ -321,6 +321,8 @@
     middle = lax.rem(lax.div(sp_at, near) + lax.div(sp_at, max(1, near // 2)), 2)
 
     def in_order(step):
+        last = token_split - 2
+        step = jnp.where(step < 2, step, 2 + lax.rem(step + near - 4 + last, last))
         return flipped(step, middle * (near // 2) * lax.div(step, near), token_split)
 
     def along(i):
@@ -534,7 +536,7 @@
         i = in_order(step)
         along(i).wait_recv()
 
-        @pl.when(step >= near)
+        @pl.when(i >= near)
         def _():
             over(i).start()
 

time: 106 us -> 104 us (0.981)
  the two profiles are of different devices: /device:TPU:3 before, /device:TPU:0 now
where the time goes in v4:
time: 104 us; the launch traced here: 103 us
  Pallas kernels  101 us (97%)
  local copies, waits for them, and re-layouts  1.77 us (2%)
    pallas_call x1, Pallas kernels, per_device(): pl.pallas_call(functools.partial(layer_kernel, token_split, capacity), ou...  101 us

profile of v4, /device:TPU:0, one launch (start us, length us, event | category | flops | bytes accessed | tf_op | source)
XLA Modules:
  0.0 102.7 jit_solution(8043628504322520009)
XLA Ops:
  0.0 100.9 %layer.1 = bf16[96,2048]{1,0:T(8,128)(2,1)} custom-call(f32[3]{0:T(128)} %sinks_ref.1, bf16[192,384]{1,0:T(8,128)(2,1)} %bitcast.6, bf16[64,384]{1,0:T(8,128)(2,1)} %bitcast.7, bf16[64,384]{1,0:T(8,128)(2,1)} %bitcast.8, f32[1,2048]{1,0:T(1,128)} %bitcast.9, s32[2,384]{1,0:T(2,128)} %bitcast.10, f32[2,96]{1,0:T(2,128)} %bitcast.11, ...), custom_call_target="tpu_custom_call" | custom-call | tf_op jit(solution)/shard_map/layer/pallas_call | solution.py:670
  100.9 1.8 %copy.18 = bf16[96,2048]{1,0:T(8,128)(2,1)} copy(bf16[96,2048]{1,0:T(8,128)(2,1)} %layer.1) | data formatting | bytes 786432

commit v5 on v4

--- a/solution.py
+++ b/solution.py
@@ -553,7 +553,6 @@
             .astype(shared_part.dtype)
             .reshape(halves, own, tile)
         )
-    shared_over.start()
     for n in range(3, 6):
         loads[n].wait()
         shares[n].wait()
@@ -590,6 +589,10 @@
                 along(i).wait_send()
                 outgoing[partner_of(i)] = summed
                 home_copy(i).start()
+
+        @pl.when(step == 0)
+        def _():
+            shared_over.start()
 
         @pl.when(step + 2 < token_split)
         def _():

time: 104 us -> 104 us (level)
  no operation moved by 1% of the time
where the time goes in v5:
time: 104 us; the launch traced here: 103 us
  Pallas kernels  101 us (97%)
  local copies, waits for them, and re-layouts  1.77 us (2%)
    pallas_call x1, Pallas kernels, per_device(): pl.pallas_call(functools.partial(layer_kernel, token_split, capacity), ou...  101 us

profile of v5, /device:TPU:0, one launch (start us, length us, event | category | flops | bytes accessed | tf_op | source)
XLA Modules:
  0.0 102.8 jit_solution(2329864147345811043)
XLA Ops:
  0.0 101.0 %layer.1 = bf16[96,2048]{1,0:T(8,128)(2,1)} custom-call(f32[3]{0:T(128)} %sinks_ref.1, bf16[192,384]{1,0:T(8,128)(2,1)} %bitcast.6, bf16[64,384]{1,0:T(8,128)(2,1)} %bitcast.7, bf16[64,384]{1,0:T(8,128)(2,1)} %bitcast.8, f32[1,2048]{1,0:T(1,128)} %bitcast.9, s32[2,384]{1,0:T(2,128)} %bitcast.10, f32[2,96]{1,0:T(2,128)} %bitcast.11, ...), custom_call_target="tpu_custom_call" | custom-call | tf_op jit(solution)/shard_map/layer/pallas_call | solution.py:673
  101.0 1.8 %copy.18 = bf16[96,2048]{1,0:T(8,128)(2,1)} copy(bf16[96,2048]{1,0:T(8,128)(2,1)} %layer.1) | data formatting | bytes 786432
